TPU v7x, 128 devices: a whole 4x4x4 slice. The times are simulated.
128 devices in a mesh: sp: 32 (over z, y, core), tp: 4 (over x).
Axes of the slice: x: 4, y: 4, z: 4, core: 2. Of those that a mesh axis runs over, the one named last changes fastest.
Arguments:
- queries: bfloat16 [16384, 2048], P('sp', 'tp'), may hold values from -6 to 6
- keys: bfloat16 [16384, 512], P('sp', 'tp'), may hold values from -6 to 6
- values: bfloat16 [16384, 512], P('sp', 'tp'), may hold values from -6 to 6
- residual: bfloat16 [16384, 2048], P(('sp', 'tp')), may hold values from -0.119628906 to 0.119628906
- out_proj: bfloat16 [2048, 2048], replicated, may hold values from -0.125 to 0.125
- query_gain: float32 [128], replicated, may hold values from 0.7 to 7
- key_gain: float32 [128], replicated, may hold values from 0.7 to 7
- norm_gain: float32 [2048], replicated, may hold values from 0.1 to 1.9
- routes: int32 [16384, 4], P(('sp', 'tp')), may hold values from 0 to 127, all different within a row; in each aligned block of 128 rows (0 to 127, 128 to 255, ...) at most 8 rows name the same one
- route_weight: float32 [16384, 4], P(('sp', 'tp')), may hold values from 0.1 to 1
- expert_gate: bfloat16 [128, 2048, 256], P(('sp', 'tp')), may hold values from -0.125 to 0.125
- expert_up: bfloat16 [128, 2048, 256], P(('sp', 'tp')), may hold values from -0.125 to 0.125
- expert_down: bfloat16 [128, 256, 2048], P(('sp', 'tp')), may hold values from -0.375 to 0.375
- shared_gate: bfloat16 [2048, 256], replicated, may hold values from -0.125 to 0.125
- shared_up: bfloat16 [2048, 256], replicated, may hold values from -0.125 to 0.125
- shared_down: bfloat16 [256, 2048], replicated, may hold values from -0.375 to 0.375
Outputs:
- layer_out: bfloat16 [16384, 2048], P(('sp', 'tp'))
Inputs may be any that keep to these rules, and one draw needn't show every extreme that they name: In the rows of one device (aligned blocks of 128 tokens), no expert is named by more than 8 routes; some expert is named by exactly 8 routes of some device; the 4 experts of a token differ.
All inputs are finite; a program needn't handle non-finite values.
Results may differ from a plain program's by a relative error of at most 0.023.
The roundings to bfloat16 on the way count: a program that leaves them out, or rounds other values in their place, can miss the bound.
Values may be sent and summed in bfloat16 or wider, within the bound.
A program may use at most 128 MiB of HBM per device.

v0:
```python
import math

import jax
import jax.numpy as jnp
from jax import lax
from jax.sharding import PartitionSpec as P

HEADS = 16
KV_HEADS = 4
GRID_W = 64


EPS = 1e-06
THETA = 10000.0


def side_by_side(arrays, axis, dim, along):
    both = jnp.concatenate(arrays, axis=along)
    result, at, outs = (lax.all_gather(both, axis, axis=dim, tiled=True), 0, [])
    for a in arrays:
        outs.append(lax.slice_in_dim(result, at, at + a.shape[along], axis=along))
        at += a.shape[along]
    return tuple(outs)


def rotate_pairs(block, cosine, sine):
    first, second = jnp.split(block, 2, axis=-1)
    return jnp.concatenate(
        [first * cosine - second * sine, second * cosine + first * sine], axis=-1
    )


def normed_rotary(source, gain, heads, offset):
    count = source.shape[0]
    width = gain.shape[0]
    values_f = source.astype(jnp.float32).reshape(count, heads, width)
    values_f = (
        values_f * lax.rsqrt(jnp.mean(values_f * values_f, axis=-1, keepdims=True) + EPS) * gain
    )
    position = offset + jnp.arange(count, dtype=jnp.int32)
    grid_row = (position // GRID_W).astype(jnp.float32)
    grid_col = (position % GRID_W).astype(jnp.float32)
    quarter = width // 4
    inverse = jnp.power(THETA, -4.0 * jnp.arange(quarter, dtype=jnp.float32) / width)
    row_angle = (grid_row[:, None] * inverse[None, :])[:, None, :]
    col_angle = (grid_col[:, None] * inverse[None, :])[:, None, :]
    row_half, col_half = jnp.split(values_f, 2, axis=-1)
    turned = jnp.concatenate(
        [
            rotate_pairs(row_half, jnp.cos(row_angle), jnp.sin(row_angle)),
            rotate_pairs(col_half, jnp.cos(col_angle), jnp.sin(col_angle)),
        ],
        axis=-1,
    )
    return turned.reshape(count, heads * width).astype(jnp.bfloat16)


def expert_apply(arrived, expert_gate, expert_up, expert_down):
    sources, slots, width = arrived.shape
    local = expert_gate.shape[0]
    grouped = arrived.reshape(sources // local, local, slots, width)
    gate_part = jnp.einsum(
        "sech,ehf->secf", grouped, expert_gate, preferred_element_type=jnp.float32
    )
    up_part = jnp.einsum("sech,ehf->secf", grouped, expert_up, preferred_element_type=jnp.float32)
    hidden_e = (jax.nn.silu(gate_part) * up_part).astype(jnp.bfloat16)
    result = jnp.einsum("secf,efh->sech", hidden_e, expert_down, preferred_element_type=jnp.float32)
    return result.astype(jnp.bfloat16).reshape(sources, slots, width)


def body(
    queries,
    keys,
    values,
    residual,
    out_proj,
    query_gain,
    key_gain,
    norm_gain,
    routes,
    route_weight,
    expert_gate,
    expert_up,
    expert_down,
    shared_gate,
    shared_up,
    shared_down,
):
    tok_local = queries.shape[0]
    width = query_gain.shape[0]
    group = HEADS // KV_HEADS
    kv_local = keys.shape[1] // width
    scale = 1.0 / math.sqrt(width)
    offset = lax.axis_index("sp") * tok_local
    q_rot = normed_rotary(queries, query_gain, kv_local * group, offset)
    k_rot = normed_rotary(keys, key_gain, kv_local, offset)
    query_3d = q_rot.reshape(tok_local, kv_local, group, width).transpose(1, 2, 0, 3)
    query_3d = query_3d.reshape(kv_local, group * tok_local, width)
    start_state = (
        jnp.full((kv_local, group * tok_local), -jnp.inf, jnp.float32),
        jnp.zeros((kv_local, group * tok_local), jnp.float32),
        jnp.zeros((kv_local, group * tok_local, width), jnp.float32),
    )
    key_piece, value_piece = side_by_side((k_rot, values), "sp", 0, 1)
    count = key_piece.shape[0]
    block = math.gcd(count, 512)

    def one_block(index_block, state):
        running_max, running_sum, accum = state
        key_rows = lax.dynamic_slice_in_dim(key_piece, index_block * block, block, 0)
        value_rows = lax.dynamic_slice_in_dim(value_piece, index_block * block, block, 0)
        key_3d = key_rows.reshape(block, kv_local, width)
        value_3d = value_rows.reshape(block, kv_local, width)
        scores = (
            jnp.einsum("gqd,kgd->gqk", query_3d, key_3d, preferred_element_type=jnp.float32) * scale
        )
        new_max = jnp.maximum(running_max, jnp.max(scores, axis=-1))
        weights = jnp.exp(scores - new_max[..., None])
        factor = jnp.exp(running_max - new_max)
        new_sum = running_sum * factor + jnp.sum(weights, axis=-1)
        added = jnp.einsum(
            "gqk,kgd->gqd",
            weights.astype(jnp.bfloat16),
            value_3d,
            preferred_element_type=jnp.float32,
        )
        return (new_max, new_sum, accum * factor[..., None] + added)

    final_max, final_sum, final_acc = lax.fori_loop(0, count // block, one_block, start_state)
    attn_local = (final_acc / final_sum[..., None]).astype(jnp.bfloat16)
    attn_local = attn_local.reshape(kv_local, group, tok_local, width).transpose(2, 0, 1, 3)
    attn_local = attn_local.reshape(tok_local, kv_local * group * width)
    all_heads = lax.all_to_all(attn_local, "tp", split_axis=0, concat_axis=1, tiled=True)
    projected = jnp.dot(all_heads, out_proj, preferred_element_type=jnp.float32)
    hidden1 = (residual.astype(jnp.float32) + projected).astype(jnp.bfloat16)
    hidden_f = hidden1.astype(jnp.float32)
    normed = (
        hidden_f
        * lax.rsqrt(jnp.mean(hidden_f * hidden_f, axis=-1, keepdims=True) + EPS)
        * norm_gain
    ).astype(jnp.bfloat16)
    rows_local = normed.shape[0]
    top_count = routes.shape[1]
    pair_count = rows_local * top_count
    expert_total = expert_gate.shape[0] * lax.axis_size("sp") * lax.axis_size("tp")
    capacity = max(2, 2 * rows_local * top_count // expert_total)
    flat_routes = routes.reshape(pair_count)
    one_hot = (flat_routes[:, None] == jnp.arange(expert_total, dtype=jnp.int32)[None, :]).astype(
        jnp.float32
    )
    lower = (jnp.arange(pair_count)[:, None] >= jnp.arange(pair_count)[None, :]).astype(jnp.float32)
    running_count = jnp.dot(lower, one_hot, precision=lax.Precision.HIGHEST)
    slot_place = (jnp.sum(running_count * one_hot, axis=1) - 1.0).astype(jnp.int32)
    slot_index = flat_routes * capacity + slot_place
    slot_total = expert_total * capacity
    placement = (jnp.arange(slot_total, dtype=jnp.int32)[:, None] == slot_index[None, :]).astype(
        jnp.bfloat16
    )
    placement = jnp.sum(placement.reshape(slot_total, rows_local, top_count), axis=2)
    send_rows = jnp.dot(placement, normed, preferred_element_type=jnp.float32).astype(jnp.bfloat16)
    send_rows = send_rows.reshape(expert_total, capacity, normed.shape[1])
    shared_hidden = (
        jax.nn.silu(jnp.dot(normed, shared_gate, preferred_element_type=jnp.float32))
        * jnp.dot(normed, shared_up, preferred_element_type=jnp.float32)
    ).astype(jnp.bfloat16)
    shared_out = jnp.dot(shared_hidden, shared_down, preferred_element_type=jnp.float32)
    processed = expert_apply(
        lax.all_to_all(send_rows, ("sp", "tp"), split_axis=0, concat_axis=0, tiled=True),
        expert_gate,
        expert_up,
        expert_down,
    )
    returned = lax.all_to_all(processed, ("sp", "tp"), split_axis=0, concat_axis=0, tiled=True)
    returned = returned.reshape(slot_total, normed.shape[1])
    routed = (
        returned[slot_index].reshape(rows_local, top_count, normed.shape[1]).astype(jnp.float32)
    )
    mixed = jnp.einsum("tk,tkd->td", route_weight, routed) + shared_out
    return (hidden_f + mixed).astype(jnp.bfloat16)


def solution(mesh):
    placed = (
        P("sp", "tp"),
        P("sp", "tp"),
        P("sp", "tp"),
        P(("sp", "tp"), None),
        P(),
        P(),
        P(),
        P(),
        P(("sp", "tp"), None),
        P(("sp", "tp"), None),
        P(("sp", "tp"), None, None),
        P(("sp", "tp"), None, None),
        P(("sp", "tp"), None, None),
        P(),
        P(),
        P(),
    )
    return jax.shard_map(
        body, mesh=mesh, in_specs=placed, out_specs=P(("sp", "tp"), None), check_vma=False
    )
```

profile of v0, /device:TPU:1, one launch (start us, length us, event | category | flops | bytes accessed | tf_op | source)
XLA Modules:
  0.0 400.1 jit_solution(8014369260818085573)
XLA Ops:
  13.8 1.9 multiply_cosine_fusion.1
  16.4 1.8 fusion.31
  20.2 53.3 %all-gather.2.cloned.1.call-done = bf16[16384,256]{0,1:T(8,128)(2,1)} async-done(((bf16[512,256]{0,1:T(8,128)(2,1)}), bf16[16384,256]{0,1:T(8,128)(2,1)}) %all-gather.2.cloned.1.call-update) | async-done | bytes 8388624 | tf_op jit(solution)/shard_map/all_gather | solution.py:19
  73.5 5.8 %fusion.69 = (bf16[16384,128]{0,1:T(8,128)(2,1)}, bf16[16384,128]{0,1:T(8,128)(2,1)}) fusion(bf16[16384,256]{0,1:T(8,128)(2,1)} %all-gather.2.cloned.1.call-done), kind=kLoop, calls=%fused_computation.125 | loop fusion | bytes 16777216 | tf_op jit(solution)/shard_map/slice | solution.py:21
  79.3 146.8 %while.18 = (s32[]{:T(128)}, f32[1,2048]{1,0:T(1,128)S(1)}, f32[1,2048]{1,0:T(1,128)S(1)}, f32[1,2048,128]{2,1,0:T(8,128)S(1)}, bf16[16384,128]{0,1:T(8,128)(2,1...) while((s32[]{:T(128)}, f32[1,2048]{1,0:T(1,128)S(1)}, ...), condition=%wide.region_5.6_spmd.clone, body=%wide.region_2.5_spmd.clone.sunk | while | flops 546056192 | bytes 15597751 | solution.py:129
  81.7 2.1 fusion.92
  83.9 1.6 multiply_reduce_fusion.4
  86.3 2.1 fusion.92
  88.5 1.6 multiply_reduce_fusion.4
  90.9 2.1 fusion.92
  93.1 1.6 multiply_reduce_fusion.4
  95.5 2.1 fusion.92
  97.7 1.6 multiply_reduce_fusion.4
  100.1 2.1 fusion.92
  102.3 1.6 multiply_reduce_fusion.4
  104.7 2.1 fusion.92
  106.9 1.6 multiply_reduce_fusion.4
  109.3 2.1 fusion.92
  111.4 1.6 multiply_reduce_fusion.4
  113.9 2.1 fusion.92
  116.0 1.6 multiply_reduce_fusion.4
  118.5 2.1 fusion.92
  120.6 1.6 multiply_reduce_fusion.4
  123.1 2.1 fusion.92
  125.2 1.6 multiply_reduce_fusion.4
  127.6 2.1 fusion.92
  129.8 1.6 multiply_reduce_fusion.4
  132.2 2.1 fusion.92
  134.4 1.6 multiply_reduce_fusion.4
  136.8 2.1 fusion.92
  139.0 1.6 multiply_reduce_fusion.4
  141.4 2.1 fusion.92
  143.6 1.6 multiply_reduce_fusion.4
  146.0 2.1 fusion.92
  148.2 1.6 multiply_reduce_fusion.4
  150.6 2.1 fusion.92
  155.2 2.1 fusion.92
  159.8 2.1 fusion.92
  164.4 2.1 fusion.92
  168.9 2.1 fusion.92
  173.5 2.1 fusion.92
  178.1 2.1 fusion.92
  182.7 2.1 fusion.92
  187.3 2.1 fusion.92
  191.9 2.1 fusion.92
  196.5 2.1 fusion.92
  201.1 2.1 fusion.92
  205.7 2.1 fusion.92
  210.3 2.1 fusion.92
  214.8 2.1 fusion.92
  219.4 2.1 fusion.92
  221.6 1.6 multiply_reduce_fusion.4
  224.0 2.1 fusion.92
  227.9 4.2 %all-to-all-start = ((bf16[4,128,512]{2,1,0:T(8,128)(2,1)}), bf16[4,128,512]{2,1,0:T(8,128)(2,1)S(1)}, u32[]{:S(2)}, u32[]{:S(2)}) async-start(bf16[4,128,512]{2,1,0:T(8,128)(2,1)} %all_to_all.20), calls=%async_computation | async-start | bytes 1048576 | tf_op jit(solution)/shard_map/all_to_all | solution.py:133
  232.6 8.8 %all-to-all-done = bf16[4,128,512]{2,1,0:T(8,128)(2,1)S(1)} async-done(((bf16[4,128,512]{2,1,0:T(8,128)(2,1)}), bf16[4,128,512]{2,1,0:T(8,128)(2,1)S(1)}, u32[]{:S(2)}, u32[]{:S(2)}) %all-to-all-start) | async-done | bytes 524320 | tf_op jit(solution)/shard_map/all_to_all | solution.py:133
  241.7 4.8 %multiply_reduce_fusion.1 = (f32[128]{0:T(128)S(1)}, f32[128,2048]{1,0:T(8,128)S(1)}) fusion(bf16[128,2048]{0,1:T(8,128)(2,1)S(1)} %bitcast.102, bf16[2048,2048]{1,0:T(8,128)(2,1)} %param.22, bf16[128,2048]{1,0:T(8,128)(2,1)} %param.21), kind=kOutput, calls=%fused_computation.47 | convolution fusion | flops 1075314560 | bytes 10486272 | tf_op jit(solution)/shard_map/dot_general | solution.py:134
  247.9 59.7 %all_to_all.29 = bf16[128,8,2048]{2,1,0:T(8,128)(2,1)S(1)} all-to-all(bf16[128,8,2048]{2,1,0:T(8,128)(2,1)S(1)} %convert_bitcast_fusion), channel_id=1, replica_groups=mesh['sp'=32,'tp'=4] {'sp','tp'}, dimensions={0} | all-to-all | bytes 8388608 | tf_op jit(solution)/shard_map/all_to_all | solution.py:168
  311.4 4.3 %copy.56 = bf16[128,8,2048]{2,1,0:T(8,128)(2,1)} copy(bf16[128,8,2048]{2,0,1:T(8,128)(2,1)S(1)} %convolution_convert_fusion) | data formatting | bytes 8388608 | tf_op jit(solution)/shard_map/convert_element_type | solution.py:68
  315.7 5.2 %all-to-all-start.2 = ((bf16[128,8,2048]{2,1,0:T(8,128)(2,1)}), bf16[128,8,2048]{2,1,0:T(8,128)(2,1)}, u32[]{:S(2)}, u32[]{:S(2)}) async-start(bf16[128,8,2048]{2,1,0:T(8,128)(2,1)} %copy.56), calls=%async_computation.2 | async-start | bytes 8388608 | tf_op jit(solution)/shard_map/all_to_all | solution.py:173
  321.6 52.5 %all-to-all-done.2 = bf16[128,8,2048]{2,1,0:T(8,128)(2,1)} async-done(((bf16[128,8,2048]{2,1,0:T(8,128)(2,1)}), bf16[128,8,2048]{2,1,0:T(8,128)(2,1)}, u32[]{:S(2)}, u32[]{:S(2)}) %all-to-all-start.2) | async-done | bytes 4194336 | tf_op jit(solution)/shard_map/all_to_all | solution.py:173
  374.0 8.0 %gather_fusion = bf16[512,2048]{1,0:T(8,128)(2,1)} fusion(bf16[1024,2048]{1,0:T(8,128)(2,1)} %bitcast.29, s32[1024]{0:T(1024)S(1)} %pad_clamp_fusion), kind=kCustom, calls=%fused_computation | custom fusion | bytes 4196352 | tf_op jit(solution)/shard_map/gather | solution.py:176
  382.0 4.2 %reshape.478 = bf16[128,4,2048]{2,1,0:T(4,128)(2,1)} reshape(bf16[512,2048]{1,0:T(8,128)(2,1)} %gather_fusion) | data formatting | bytes 4194304 | tf_op jit(solution)/shard_map/reshape | solution.py:176
  386.2 3.8 fusion.70
  390.0 3.3 fusion.19
  (203 shorter events, 68.9 us)
Async XLA Ops:
  6.5 303.6 %copy-start = (bf16[1,256,2048]{2,1,0:T(8,128)(2,1)S(1)}, bf16[1,256,2048]{2,1,0:T(8,128)(2,1)}, u32[]{:S(2)}) copy-start(bf16[1,256,2048]{2,1,0:T(8,128)(2,1)} %param.30) | copy-start | bytes 3145732
  6.5 9.2 %copy-start.5 = (f32[128]{0:T(128)S(1)}, f32[128]{0:T(128)}, u32[]{:S(2)}) copy-start(f32[128]{0:T(128)} %param.23) | copy-start | bytes 1540
  6.5 67.0 %all-gather.2.cloned.1.call-start = ((), (), s32[]{:S(2)}) async-start(), calls=%async_computation.3 | async-start | bytes 8650752 | tf_op jit(solution)/shard_map/all_gather | solution.py:19
  227.9 13.5 %all-to-all-start = ((bf16[4,128,512]{2,1,0:T(8,128)(2,1)}), bf16[4,128,512]{2,1,0:T(8,128)(2,1)S(1)}, u32[]{:S(2)}, u32[]{:S(2)}) async-start(bf16[4,128,512]{2,1,0:T(8,128)(2,1)} %all_to_all.20), calls=%async_computation | async-start | bytes 1048576 | tf_op jit(solution)/shard_map/all_to_all | solution.py:133
  241.7 4.8 %copy-start.3 = (f32[2048]{0:T(1024)S(1)}, f32[2048]{0:T(1024)}, u32[]{:S(2)}) copy-start(f32[2048]{0:T(1024)} %param.25) | copy-start | bytes 24580
  247.9 59.7 %copy-start.6 = (bf16[1,2048,256]{2,1,0:T(8,128)(2,1)S(1)}, bf16[1,2048,256]{2,1,0:T(8,128)(2,1)}, u32[]{:S(2)}) copy-start(bf16[1,2048,256]{2,1,0:T(8,128)(2,1)} %param.28) | copy-start | bytes 3145732
  307.6 1.3 copy-start.7
  315.7 5.3 %copy-start.4 = (f32[128,4]{0,1:T(4,128)S(1)}, f32[128,4]{0,1:T(4,128)}, u32[]{:S(2)}) copy-start(f32[128,4]{0,1:T(4,128)} %param.27) | copy-start | bytes 6148
  315.7 5.5 %copy-start.2 = (bf16[2048,256]{1,0:T(8,128)(2,1)S(1)}, bf16[2048,256]{1,0:T(8,128)(2,1)}, u32[]{:S(2)}) copy-start(bf16[2048,256]{1,0:T(8,128)(2,1)} %param.31) | copy-start | bytes 3145732
  315.7 58.3 %all-to-all-start.2 = ((bf16[128,8,2048]{2,1,0:T(8,128)(2,1)}), bf16[128,8,2048]{2,1,0:T(8,128)(2,1)}, u32[]{:S(2)}, u32[]{:S(2)}) async-start(bf16[128,8,2048]{2,1,0:T(8,128)(2,1)} %copy.56), calls=%async_computation.2 | async-start | bytes 8388608 | tf_op jit(solution)/shard_map/all_to_all | solution.py:173
  382.0 8.0 %copy-start.1 = (bf16[256,2048]{1,0:T(8,128)(2,1)S(1)}, bf16[256,2048]{1,0:T(8,128)(2,1)}, u32[]{:S(2)}) copy-start(bf16[256,2048]{1,0:T(8,128)(2,1)} %param.33) | copy-start | bytes 3145732
Sparse Core Ops, SparseCore 0:
  10.9 62.5 all-gather.1
where the time goes:
time: 402 us; the launch traced here: 400 us
  matrix products  138 us (34%)
  waiting for transfers between devices  115 us (29%)
  blocking collectives  59.7 us (15%)
  other arithmetic  33.8 us (8%)
  local copies, waits for them, and re-layouts  28.9 us (7%)
  between operations  13.7 us (3%)
  starting transfers between devices  9.41 us (2%)
    dot_general x32, matrix products, one_block(): jnp.einsum('gqk,kgd->gqd', weights.astype(jnp.bfloat16), value_3d, prefer...  67.9 us
    all_to_all x1, blocking collectives, body(): lax.all_to_all(send_rows, ('sp', 'tp'), split_axis=0, concat_axis=0, tile...  59.7 us
    all_gather x1, waiting for transfers between devices, side_by_side(): result, at, outs = (lax.all_gather(both, axis, axis=dim, tiled=True), 0, [])  53.3 us
    dot_general x32, matrix products, one_block(): jnp.einsum('gqd,kgd->gqk', query_3d, key_3d, preferred_element_type=jnp.f...  52.7 us
    all_to_all x1, waiting for transfers between devices, body(): lax.all_to_all(processed, ('sp', 'tp'), split_axis=0, concat_axis=0, tile...  52.5 us
    reduce_sum x32, other arithmetic, one_block(): new_sum = running_sum * factor + jnp.sum(weights, axis=-1)  22.7 us
    all_to_all x1, waiting for transfers between devices, body(): lax.all_to_all(attn_local, 'tp', split_axis=0, concat_axis=1, tiled=True)  8.83 us
  transfers between devices with their start and end apart: 3, of which 3 were waited for; matrix products, arithmetic and copies ran while one was open for 3% of the time, Pallas kernels for 0%

commit v1 on v0

v1 whole, which is shorter than its diff:
```python
import functools
import math

import jax
import jax.numpy as jnp
import numpy as np
from jax import lax
from jax.experimental import pallas as pl
from jax.experimental.pallas import tpu as pltpu
from jax.sharding import PartitionSpec as P

HEADS = 16
KV_HEADS = 4
GRID_W = 64
HD = 128
TOK = 512
EPS = 1e-06
THETA = 10000.0
MESH = pl.DeviceIdType.MESH
F32 = jnp.float32
BF16 = jnp.bfloat16


def rotary_tables():
    quarter = HD // 4
    inverse = (THETA ** (-4.0 * np.arange(quarter, dtype=np.float64) / HD)).astype(np.float32)

    def table(count):
        angle = np.arange(count, dtype=np.float32)[:, None] * inverse[None, :]
        angle = angle.astype(np.float32).astype(np.float64)
        cosine = np.cos(angle).astype(np.float32)
        sine = np.sin(angle).astype(np.float32)
        return np.concatenate([cosine, cosine], 1), np.concatenate([-sine, sine], 1)

    row_cos, row_sin = table(256)
    col_cos, col_sin = table(GRID_W)
    zr, zc = np.zeros_like(row_cos), np.zeros_like(col_cos)
    rows = np.stack([np.concatenate([row_cos, zr], 1), np.concatenate([row_sin, zr], 1)])
    cols = np.stack([np.concatenate([zc, col_cos], 1), np.concatenate([zc, col_sin], 1)])
    return rows, cols


def normed_rotary(source, gain, cos_t, sin_t):
    x = source.astype(F32)
    x = x * lax.rsqrt(jnp.mean(x * x, axis=-1, keepdims=True) + EPS) * gain
    lane = lax.broadcasted_iota(jnp.int32, x.shape, 1)
    partner = jnp.where((lane // 32) % 2 == 0, pltpu.roll(x, 96, 1), pltpu.roll(x, 32, 1))
    return x * cos_t + partner * sin_t


A_SET = ((1, 0), (3, 0), (0, 1), (0, 3))
B_SET = ((1, 1), (1, 3), (3, 1), (3, 3))
C_SET = ((2, 0), (0, 2))
D_SET = ((2, 1), (2, 3), (1, 2), (3, 2))
E_SET = ((2, 2),)


def attention_kernel(
    q_ref,
    k_ref,
    v_ref,
    qg_ref,
    kg_ref,
    rows_ref,
    cols_ref,
    hx_ref,
    kt_all,
    v_all,
    q_hl,
    trig,
    acc,
    mstate,
    o_tok,
    send_sem,
    krecv,
    vrecv,
    xrecv,
):
    sp = lax.axis_index("sp")
    tx = lax.axis_index("tp")
    core = sp % 2
    yy = (sp // 2) % 4
    zz = sp // 8

    def at(y, z, c):
        return (z % 4) * 8 + (y % 4) * 2 + c

    sib = at(yy, zz, 1 - core)
    y_next, y_prev = at(yy + 1, zz, core), at(yy + 3, zz, core)
    z_next, z_prev = at(yy, zz + 1, core), at(yy, zz + 3, core)

    barrier = pltpu.get_barrier_semaphore()
    for peer in (sib, y_next, y_prev, z_next, z_prev):
        pl.semaphore_signal(barrier, inc=1, device_id=(peer, tx), device_id_type=MESH)
    for step in (1, 2, 3):
        pl.semaphore_signal(
            barrier, inc=1, device_id=(sp, (tx + step) % 4), device_id_type=MESH
        )

    counter = [0]
    sent = []

    def push(kind, slot, peer):
        buf, recv = (kt_all, krecv) if kind == 0 else (v_all, vrecv)
        copy = pltpu.make_async_remote_copy(
            src_ref=buf.at[slot],
            dst_ref=buf.at[slot],
            send_sem=send_sem.at[counter[0]],
            recv_sem=recv.at[slot],
            device_id=(peer, tx),
            device_id_type=MESH,
        )
        sent.append((kind, counter[0]))
        counter[0] += 1
        copy.start()

    def arrived(kind, slot):
        buf, recv = (kt_all, krecv) if kind == 0 else (v_all, vrecv)
        pltpu.make_async_remote_copy(
            src_ref=buf.at[slot],
            dst_ref=buf.at[slot],
            send_sem=send_sem.at[0],
            recv_sem=recv.at[slot],
            device_id=(sib, tx),
            device_id_type=MESH,
        ).wait_recv()

    def origin(dy, dz, c):
        return at(yy - dy + 4, zz - dz + 4, c)

    for r in range(8):
        sl = pl.ds(r * GRID_W, GRID_W)
        for i in range(2):
            trig[i, sl, :] = rows_ref[i, pl.ds(sp * 8 + r, 1), :] + cols_ref[i]

    kr = normed_rotary(k_ref[...], kg_ref[...], trig[0], trig[1])
    kt_all[sp] = kr.T.astype(BF16)
    v_all[sp] = v_ref[...]
    pl.semaphore_wait(barrier, 8)
    for kind in (0, 1):
        for peer in (y_next, y_prev, z_next, z_prev):
            push(kind, sp, peer)
    push(0, sp, sib)
    push(1, sp, sib)

    factor = math.log2(math.e) / math.sqrt(HD)
    for h in range(4):
        qr = normed_rotary(q_ref[:, h * HD : (h + 1) * HD], qg_ref[...], trig[0], trig[1])
        qs = qr.astype(BF16).astype(F32) * factor
        hi = qs.astype(BF16)
        q_hl[h * TOK : (h + 1) * TOK, 0:HD] = hi
        q_hl[h * TOK : (h + 1) * TOK, HD : 2 * HD] = (qs - hi.astype(F32)).astype(BF16)
    acc[...] = jnp.zeros_like(acc)
    mstate[...] = jnp.full_like(mstate, -1e30)

    def attend(slots):
        n = len(slots)
        width = n * TOK
        kt = jnp.concatenate([kt_all[s] for s in slots], axis=1)
        k2 = jnp.concatenate([kt, kt], axis=0)
        vv = jnp.concatenate([v_all[s] for s in slots], axis=0)
        v2 = jnp.concatenate([vv, jnp.ones_like(vv)], axis=1)

        def scores(h):
            return jnp.dot(
                q_hl[h * TOK : (h + 1) * TOK, :], k2, preferred_element_type=F32
            )

        s = scores(0)
        for h in range(4):
            sl = slice(h * TOK, (h + 1) * TOK)
            old = mstate[sl, :]
            top = s[:, 0:HD]
            for j in range(1, width // HD):
                top = jnp.maximum(top, s[:, j * HD : (j + 1) * HD])
            new = jnp.maximum(old, jnp.max(top, axis=1, keepdims=True))
            mstate[sl, :] = new
            p = jnp.exp2(s - new[:, 0:1]).astype(BF16)
            if h < 3:
                s = scores(h + 1)
            shrink = jnp.exp2(old - new)
            pv = jnp.dot(p, v2, preferred_element_type=F32)
            acc[sl, :] = acc[sl, :] * jnp.concatenate([shrink, shrink], axis=1) + pv

    def pair_arrived(dy, dz, c):
        slot = origin(dy, dz, c)
        arrived(0, slot)
        arrived(1, slot)

    def to_sibling(group):
        for dy, dz in group:
            slot = origin(dy, dz, core)
            push(0, slot, sib)
            push(1, slot, sib)

    arrived(0, sib)
    arrived(1, sib)
    attend([sp, sib])

    def event(t):
        if t == 0:
            for dy, dz in A_SET:
                pair_arrived(dy, dz, core)
            turn = 1 + 2 * core
            for d in (1, 3):
                push(0, origin(d, 0, core), z_next)
                push(0, origin(d, 0, core), z_prev)
                push(1, origin(0, d, core), y_next)
                push(1, origin(0, d, core), y_prev)
            push(0, origin(turn, 0, core), at(yy + turn, zz, core))
            push(1, origin(0, turn, core), at(yy, zz + turn, core))
            push(0, origin(0, 1, core), z_next)
            push(1, origin(1, 0, core), y_next)
            to_sibling(A_SET)
        if t == 1:
            for dy, dz in A_SET:
                pair_arrived(dy, dz, 1 - core)
        if t == 2:
            for dy, dz in B_SET + C_SET:
                pair_arrived(dy, dz, core)
            push(0, origin(2, 0, core), z_next)
            push(0, origin(2, 0, core), z_prev)
            push(1, origin(0, 2, core), y_next)
            push(1, origin(0, 2, core), y_prev)
            push(0, origin(1, 1, core), z_next)
            push(0, origin(3, 3, core), z_prev)
            push(1, origin(1, 1, core), y_next)
            push(1, origin(3, 3, core), y_prev)
            to_sibling(B_SET + C_SET)
        if t == 3:
            for dy, dz in B_SET:
                pair_arrived(dy, dz, 1 - core)
        if t == 4:
            for dy, dz in D_SET:
                pair_arrived(dy, dz, core)
            push(0, origin(2, 3, core), z_prev)
            push(1, origin(3, 2, core), y_prev)
            to_sibling(D_SET)
            for dy, dz in C_SET:
                pair_arrived(dy, dz, 1 - core)
        if t == 5:
            pair_arrived(2, 2, core)
            to_sibling(E_SET)
        if t == 6:
            for dy, dz in D_SET:
                pair_arrived(dy, dz, 1 - core)

    groups = (
        [(dy, dz, 0) for dy, dz in A_SET],
        [(dy, dz, 1) for dy, dz in A_SET],
        [(dy, dz, 0) for dy, dz in B_SET],
        [(dy, dz, 1) for dy, dz in B_SET],
        [(2, 0, 0), (0, 2, 0), (2, 0, 1), (0, 2, 1)],
        [(dy, dz, 0) for dy, dz in D_SET],
        [(dy, dz, 1) for dy, dz in D_SET],
    )

    def chosen(values, t):
        code = sum(v * 4**i for i, v in enumerate(values))
        out = (code >> (2 * t)) % 4
        return out

    def one_step(t, carry):
        for i in range(7):

            @pl.when(t == i)
            def _(i=i):
                event(i)

        slots = []
        for j in range(4):
            dy = chosen([g[j][0] for g in groups], t)
            dz = chosen([g[j][1] for g in groups], t)
            flip = chosen([g[j][2] for g in groups], t)
            slots.append(origin(dy, dz, (core + flip) % 2))
        attend(slots)
        return carry

    lax.fori_loop(0, 7, one_step, 0)
    pair_arrived(2, 2, 1 - core)
    attend([origin(2, 2, core), origin(2, 2, 1 - core)])

    for h in range(4):
        sl = slice(h * TOK, (h + 1) * TOK)
        o = (acc[sl, 0:HD] / acc[sl, HD : 2 * HD]).astype(BF16)
        for j in range(4):
            o_tok[j, :, h * HD : (h + 1) * HD] = o[j * 128 : (j + 1) * 128, :]
    exchanges = []
    for step in (1, 2, 3):
        peer = (tx + step) % 4
        copy = pltpu.make_async_remote_copy(
            src_ref=o_tok.at[peer],
            dst_ref=hx_ref.at[tx],
            send_sem=send_sem.at[counter[0]],
            recv_sem=xrecv.at[tx],
            device_id=(sp, peer),
            device_id_type=MESH,
        )
        counter[0] += 1
        copy.start()
        exchanges.append(copy)
    hx_ref[tx] = o_tok[tx]
    for step in (1, 2, 3):
        source = (tx + step) % 4
        pltpu.make_async_remote_copy(
            src_ref=o_tok.at[source],
            dst_ref=hx_ref.at[source],
            send_sem=send_sem.at[0],
            recv_sem=xrecv.at[source],
            device_id=(sp, source),
            device_id_type=MESH,
        ).wait_recv()
    for copy in exchanges:
        copy.wait_send()
    for kind, index in sent:
        buf, recv = (kt_all, krecv) if kind == 0 else (v_all, vrecv)
        pltpu.make_async_remote_copy(
            src_ref=buf.at[sp],
            dst_ref=buf.at[sp],
            send_sem=send_sem.at[index],
            recv_sem=recv.at[sp],
            device_id=(sib, tx),
            device_id_type=MESH,
        ).wait_send()


def attention(queries, keys, values, query_gain, key_gain):
    rows, cols = rotary_tables()
    vmem = pl.BlockSpec(memory_space=pltpu.VMEM)
    return pl.pallas_call(
        attention_kernel,
        out_shape=jax.ShapeDtypeStruct((4, 128, 512), BF16),
        in_specs=[vmem] * 7,
        out_specs=vmem,
        scratch_shapes=[
            pltpu.VMEM((32, HD, TOK), BF16),
            pltpu.VMEM((32, TOK, HD), BF16),
            pltpu.VMEM((4 * TOK, 2 * HD), BF16),
            pltpu.VMEM((2, TOK, HD), F32),
            pltpu.VMEM((4 * TOK, 2 * HD), F32),
            pltpu.VMEM((4 * TOK, HD), F32),
            pltpu.VMEM((4, 128, 4 * HD), BF16),
            pltpu.SemaphoreType.DMA((72,)),
            pltpu.SemaphoreType.DMA((32,)),
            pltpu.SemaphoreType.DMA((32,)),
            pltpu.SemaphoreType.DMA((4,)),
        ],
        compiler_params=pltpu.CompilerParams(
            collective_id=0, has_side_effects=True, vmem_limit_bytes=56 * 2**20
        ),
        name="attention",
    )(
        queries,
        keys,
        values,
        query_gain.reshape(1, HD),
        key_gain.reshape(1, HD),
        jnp.asarray(rows),
        jnp.asarray(cols),
    )


def expert_apply(arrived, expert_gate, expert_up, expert_down):
    sources, slots, width = arrived.shape
    local = expert_gate.shape[0]
    grouped = arrived.reshape(sources // local, local, slots, width)
    gate_part = jnp.einsum("sech,ehf->secf", grouped, expert_gate, preferred_element_type=F32)
    up_part = jnp.einsum("sech,ehf->secf", grouped, expert_up, preferred_element_type=F32)
    hidden_e = (jax.nn.silu(gate_part) * up_part).astype(BF16)
    result = jnp.einsum("secf,efh->sech", hidden_e, expert_down, preferred_element_type=F32)
    return result.astype(BF16).reshape(sources, slots, width)


def body(
    queries,
    keys,
    values,
    residual,
    out_proj,
    query_gain,
    key_gain,
    norm_gain,
    routes,
    route_weight,
    expert_gate,
    expert_up,
    expert_down,
    shared_gate,
    shared_up,
    shared_down,
):
    heads_x = attention(queries, keys, values, query_gain, key_gain)
    all_heads = heads_x.transpose(1, 0, 2).reshape(128, 2048)
    projected = jnp.dot(all_heads, out_proj, preferred_element_type=F32)
    hidden1 = (residual.astype(F32) + projected).astype(BF16)
    hidden_f = hidden1.astype(F32)
    normed = (
        hidden_f
        * lax.rsqrt(jnp.mean(hidden_f * hidden_f, axis=-1, keepdims=True) + EPS)
        * norm_gain
    ).astype(BF16)
    rows_local = normed.shape[0]
    top_count = routes.shape[1]
    pair_count = rows_local * top_count
    expert_total = expert_gate.shape[0] * lax.axis_size("sp") * lax.axis_size("tp")
    capacity = 8
    flat_routes = routes.reshape(pair_count)
    one_hot = (flat_routes[:, None] == jnp.arange(expert_total, dtype=jnp.int32)[None, :]).astype(
        F32
    )
    lower = (jnp.arange(pair_count)[:, None] >= jnp.arange(pair_count)[None, :]).astype(F32)
    running_count = jnp.dot(lower, one_hot, precision=lax.Precision.HIGHEST)
    slot_place = (jnp.sum(running_count * one_hot, axis=1) - 1.0).astype(jnp.int32)
    slot_index = flat_routes * capacity + slot_place
    slot_total = expert_total * capacity
    placement = (jnp.arange(slot_total, dtype=jnp.int32)[:, None] == slot_index[None, :]).astype(
        BF16
    )
    placement = jnp.sum(placement.reshape(slot_total, rows_local, top_count), axis=2)
    send_rows = jnp.dot(placement, normed, preferred_element_type=F32).astype(BF16)
    send_rows = send_rows.reshape(expert_total, capacity, normed.shape[1])
    shared_hidden = (
        jax.nn.silu(jnp.dot(normed, shared_gate, preferred_element_type=F32))
        * jnp.dot(normed, shared_up, preferred_element_type=F32)
    ).astype(BF16)
    shared_out = jnp.dot(shared_hidden, shared_down, preferred_element_type=F32)
    processed = expert_apply(
        lax.all_to_all(send_rows, ("sp", "tp"), split_axis=0, concat_axis=0, tiled=True),
        expert_gate,
        expert_up,
        expert_down,
    )
    returned = lax.all_to_all(processed, ("sp", "tp"), split_axis=0, concat_axis=0, tiled=True)
    returned = returned.reshape(slot_total, normed.shape[1])
    routed = returned[slot_index].reshape(rows_local, top_count, normed.shape[1]).astype(F32)
    mixed = jnp.einsum("tk,tkd->td", route_weight, routed) + shared_out
    return (hidden_f + mixed).astype(BF16)


def solution(mesh):
    placed = (
        P("sp", "tp"),
        P("sp", "tp"),
        P("sp", "tp"),
        P(("sp", "tp"), None),
        P(),
        P(),
        P(),
        P(),
        P(("sp", "tp"), None),
        P(("sp", "tp"), None),
        P(("sp", "tp"), None, None),
        P(("sp", "tp"), None, None),
        P(("sp", "tp"), None, None),
        P(),
        P(),
        P(),
    )
    return jax.shard_map(
        body, mesh=mesh, in_specs=placed, out_specs=P(("sp", "tp"), None), check_vma=False
    )
```

time: 402 us -> 219 us (0.54)
  matrix products: 138 us -> 17.6 us
  Pallas kernels: 0 us -> 62.7 us
  waiting for transfers between devices: 115 us -> 52.5 us
  other arithmetic: 33.8 us -> 0.3 us
  between operations: 13.7 us -> 0.2 us
  local copies, waits for them, and re-layouts: 28.9 us -> 19.2 us
  starting transfers between devices: 9.41 us -> 5.18 us
    dot_general x69 -> x5, matrix products: 132 us -> 11 us  [the longest x1 4.74 us: body(): projected = jnp.dot(all_heads, out_proj, preferred_element_type=F32)]
    pallas_call x0 -> x1, Pallas kernels: none -> 62.7 us  [attention(): pl.pallas_call(attention_kernel, out_shape=jax.ShapeDtypeStruct((4, 128,...]
    all_gather x1 -> x0, waiting for transfers between devices: 53.3 us -> none  [side_by_side(): result, at, outs = (lax.all_gather(both, axis, axis=dim, tiled=True), 0, [])]
    reduce_sum x34 -> x0, other arithmetic: 23.4 us -> none  [the longest x32 22.7 us: one_block(): new_sum = running_sum * factor + jnp.sum(weights, axis=-1)]
    all_to_all x1 -> x0, waiting for transfers between devices: 8.83 us -> none  [body(): lax.all_to_all(attn_local, 'tp', split_axis=0, concat_axis=1, tiled=True)]
    slice x1 -> x0, local copies, waits for them, and re-layouts: 5.78 us -> none  [side_by_side(): outs.append(lax.slice_in_dim(result, at, at + a.shape[along], axis=along))]
    all_to_all x1 -> x0, starting transfers between devices: 4.22 us -> none  [body(): lax.all_to_all(attn_local, 'tp', split_axis=0, concat_axis=1, tiled=True)]
  transfers between devices with their start and end apart: 3 -> 1, of which waited for: 3 -> 1; matrix products, arithmetic and copies ran while one was open for 3% -> 0% of each run, Pallas kernels for 0% -> 0%
where the time goes in v1:
time: 219 us; the launch traced here: 218 us
  Pallas kernels  62.7 us (29%)
  blocking collectives  60.8 us (28%)
  waiting for transfers between devices  52.5 us (24%)
  local copies, waits for them, and re-layouts  19.2 us (9%)
  matrix products  17.6 us (8%)
  starting transfers between devices  5.18 us (2%)
    pallas_call x1, Pallas kernels, attention(): pl.pallas_call(attention_kernel, out_shape=jax.ShapeDtypeStruct((4, 128,...  62.7 us
    all_to_all x1, blocking collectives, body(): lax.all_to_all(send_rows, ('sp', 'tp'), split_axis=0, concat_axis=0, tile...  60.8 us
    all_to_all x1, waiting for transfers between devices, body(): lax.all_to_all(processed, ('sp', 'tp'), split_axis=0, concat_axis=0, tile...  52.5 us
    gather x1, local copies, waits for them, and re-layouts, body(): returned[slot_index].reshape(rows_local, top_count, normed.shape[1])  7.98 us
    all_to_all x1, starting transfers between devices, body(): lax.all_to_all(processed, ('sp', 'tp'), split_axis=0, concat_axis=0, tile...  5.18 us
    dot_general x1, matrix products, body(): projected = jnp.dot(all_heads, out_proj, preferred_element_type=F32)  4.74 us
  transfers between devices with their start and end apart: 1, of which 1 were waited for; matrix products, arithmetic and copies ran while one was open for 0% of the time, Pallas kernels for 0%

profile of v1, /device:TPU:1, one launch (start us, length us, event | category | flops | bytes accessed | tf_op | source)
XLA Modules:
  0.0 218.3 jit_solution(3152685367684713628)
XLA Ops:
  0.0 0.0 copy-start
  0.0 0.0 copy-start.3
  0.0 0.9 copy.33
  0.9 0.1 eq.30
  1.0 0.3 fusion.8
  1.3 0.1 convert_element_type.63
  1.5 0.1 copy.35
  1.5 0.3 fusion.10
  1.8 62.7 %attention.1 = bf16[4,128,512]{2,1,0:T(8,128)(2,1)} custom-call(bf16[512,512]{1,0:T(8,128)(2,1)} %q_ref.1, bf16[512,128]{1,0:T(8,128)(2,1)} %k_ref.1, bf16[512,128]{1,0:T(8,128)(2,1)} %v_ref.1, f32[1,128]{1,0:T(1,128)} %bitcast.59, f32[1,128]{1,0:T(1,128)} %bitcast.60, f32[2,256,128]{2,1,0:T(8,128)} %constant.28.clone.rows_ref, ...), custom_call_target="tpu_custom_call" | custom-call | tf_op jit(solution)/shard_map/attention/pallas_call | solution.py:330
  64.5 1.3 copy.32
  65.8 0.0 copy-done.3
  65.8 0.0 copy-start.4
  65.8 4.7 %multiply_reduce_fusion = (f32[128]{0:T(128)S(1)}, f32[128,2048]{1,0:T(8,128)S(1)}) fusion(bf16[128,2048]{0,1:T(8,128)(2,1)S(1)} %bitcast.54, bf16[2048,2048]{1,0:T(8,128)(2,1)} %param.22, bf16[128,2048]{1,0:T(8,128)(2,1)S(1)} %copy-done.3), kind=kOutput, calls=%fused_computation.25 | convolution fusion | flops 1075314560 | bytes 10486272 | tf_op jit(solution)/shard_map/dot_general | solution.py:394
  70.6 0.0 copy-done.4
  70.6 1.3 convert_bitcast_fusion
  71.9 0.0 copy-start.6
  71.9 60.8 %all_to_all.10 = bf16[128,8,2048]{2,1,0:T(8,128)(2,1)S(1)} all-to-all(bf16[128,8,2048]{2,1,0:T(8,128)(2,1)S(1)} %convert_bitcast_fusion), channel_id=1, replica_groups=mesh['sp'=32,'tp'=4] {'sp','tp'}, dimensions={0} | all-to-all | bytes 8388608 | tf_op jit(solution)/shard_map/all_to_all | solution.py:428
  132.7 0.0 copy-done.6
  132.7 0.0 copy-start.7
  132.7 1.2 convolution_bitcast_fusion.1
  134.0 0.0 copy-done.7
  134.0 1.3 fusion.7
  135.2 0.0 copy-done
  135.2 1.3 convolution_convert_fusion
  136.5 4.3 %copy.37 = bf16[128,8,2048]{2,1,0:T(8,128)(2,1)} copy(bf16[128,8,2048]{2,0,1:T(8,128)(2,1)S(1)} %convolution_convert_fusion) | data formatting | bytes 8388608 | tf_op jit(solution)/shard_map/convert_element_type | solution.py:371
  140.8 0.0 copy-start.5
  140.8 0.0 copy-start.2
  140.8 5.2 %all-to-all-start.1 = ((bf16[128,8,2048]{2,1,0:T(8,128)(2,1)}), bf16[128,8,2048]{2,1,0:T(8,128)(2,1)}, u32[]{:S(2)}, u32[]{:S(2)}) async-start(bf16[128,8,2048]{2,1,0:T(8,128)(2,1)} %copy.37), calls=%async_computation.1 | async-start | bytes 8388608 | tf_op jit(solution)/shard_map/all_to_all | solution.py:433
  146.0 0.1 mul.66
  146.1 0.0 copy-done.5
  146.1 0.2 copy.38
  146.3 0.0 copy-done.2
  146.3 0.4 fusion.24
  146.6 52.5 %all-to-all-done.1 = bf16[128,8,2048]{2,1,0:T(8,128)(2,1)} async-done(((bf16[128,8,2048]{2,1,0:T(8,128)(2,1)}), bf16[128,8,2048]{2,1,0:T(8,128)(2,1)}, u32[]{:S(2)}, u32[]{:S(2)}) %all-to-all-start.1) | async-done | bytes 4194336 | tf_op jit(solution)/shard_map/all_to_all | solution.py:433
  199.1 8.0 %gather_fusion = bf16[512,2048]{1,0:T(8,128)(2,1)} fusion(bf16[1024,2048]{1,0:T(8,128)(2,1)} %bitcast.20, s32[1024]{0:T(1024)S(1)} %pad_clamp_fusion), kind=kCustom, calls=%fused_computation | custom fusion | bytes 4196352 | tf_op jit(solution)/shard_map/gather | solution.py:435
  207.1 0.0 copy-start.1
  207.1 4.2 %reshape.119 = bf16[128,4,2048]{2,1,0:T(4,128)(2,1)} reshape(bf16[512,2048]{1,0:T(8,128)(2,1)} %gather_fusion) | data formatting | bytes 4194304 | tf_op jit(solution)/shard_map/reshape | solution.py:435
  211.2 3.8 %fusion.25 = f32[128,1,2048]{2,1,0:T(1,128)} fusion(bf16[128,4,2048]{2,1,0:T(4,128)(2,1)} %reshape.119, bf16[128,4,1]{1,2,0:T(2,128)(2,1)S(1)} %copy.38), kind=kOutput, calls=%fused_computation.44 | convolution fusion | flops 2097152 | bytes 3146752 | tf_op jit(solution)/shard_map/tk,tkd->td/dot_general | solution.py:436
  215.1 0.0 copy-done.1
  215.1 3.3 %fusion.3 = bf16[128,2048]{1,0:T(8,128)(2,1)} fusion(f32[128,2048]{1,0:T(8,128)S(1)} %get-tuple-element.8, bf16[256,2048]{1,0:T(8,128)(2,1)S(1)} %copy-done.1, bf16[2048,256]{1,0:T(8,128)(2,1)} %param.32, f32[128,1,2048]{2,1,0:T(1,128)} %fusion.25, f32[128,256]{1,0:T(8,128)S(1)} %fusion.24, f32[2048]{0:T(1024)S(1)} %copy-done.4, f32[128]{0:T(128)S(1)} %add_rsqrt_fusion), kind=kOutput, calls=%fused_computation.8 | convolution fusion | flops 270204928 | bytes 4858368 | tf_op jit(solution)/shard_map/dot_general | solution.py:426
  (5 shorter events, 0.0 us)
Async XLA Ops:
  0.0 135.2 %copy-start = (bf16[1,256,2048]{2,1,0:T(8,128)(2,1)S(1)}, bf16[1,256,2048]{2,1,0:T(8,128)(2,1)}, u32[]{:S(2)}) copy-start(bf16[1,256,2048]{2,1,0:T(8,128)(2,1)} %param.30) | copy-start | bytes 3145732
  0.0 65.8 %copy-start.3 = (bf16[128,2048]{1,0:T(8,128)(2,1)S(1)}, bf16[128,2048]{1,0:T(8,128)(2,1)}, u32[]{:S(2)}) copy-start(bf16[128,2048]{1,0:T(8,128)(2,1)} %param.21) | copy-start | bytes 1572868
  65.8 4.8 %copy-start.4 = (f32[2048]{0:T(1024)S(1)}, f32[2048]{0:T(1024)}, u32[]{:S(2)}) copy-start(f32[2048]{0:T(1024)} %param.25) | copy-start | bytes 24580
  71.9 60.8 %copy-start.6 = (bf16[1,2048,256]{2,1,0:T(8,128)(2,1)S(1)}, bf16[1,2048,256]{2,1,0:T(8,128)(2,1)}, u32[]{:S(2)}) copy-start(bf16[1,2048,256]{2,1,0:T(8,128)(2,1)} %param.28) | copy-start | bytes 3145732
  132.7 1.3 copy-start.7
  140.8 5.3 %copy-start.5 = (f32[128,4]{0,1:T(4,128)S(1)}, f32[128,4]{0,1:T(4,128)}, u32[]{:S(2)}) copy-start(f32[128,4]{0,1:T(4,128)} %param.27) | copy-start | bytes 6148
  140.8 5.5 %copy-start.2 = (bf16[2048,256]{1,0:T(8,128)(2,1)S(1)}, bf16[2048,256]{1,0:T(8,128)(2,1)}, u32[]{:S(2)}) copy-start(bf16[2048,256]{1,0:T(8,128)(2,1)} %param.31) | copy-start | bytes 3145732
  140.8 58.3 %all-to-all-start.1 = ((bf16[128,8,2048]{2,1,0:T(8,128)(2,1)}), bf16[128,8,2048]{2,1,0:T(8,128)(2,1)}, u32[]{:S(2)}, u32[]{:S(2)}) async-start(bf16[128,8,2048]{2,1,0:T(8,128)(2,1)} %copy.37), calls=%async_computation.1 | async-start | bytes 8388608 | tf_op jit(solution)/shard_map/all_to_all | solution.py:433
  207.1 8.0 %copy-start.1 = (bf16[256,2048]{1,0:T(8,128)(2,1)S(1)}, bf16[256,2048]{1,0:T(8,128)(2,1)}, u32[]{:S(2)}) copy-start(bf16[256,2048]{1,0:T(8,128)(2,1)} %param.33) | copy-start | bytes 3145732

commit v2 on v1

--- a/solution.py
+++ b/solution.py
@@ -1,4 +1,3 @@
-import functools
 import math
 
 import jax
@@ -55,7 +54,10 @@
 E_SET = ((2, 2),)
 
 
-def attention_kernel(
+COLS = ((0, 640), (640, 1280), (1280, 2048))
+
+
+def layer_kernel(
     q_ref,
     k_ref,
     v_ref,
@@ -63,6 +65,18 @@
     kg_ref,
     rows_ref,
     cols_ref,
+    ng_ref,
+    routes_ref,
+    rweight_ref,
+    residual_hbm,
+    out_proj_hbm,
+    gate_hbm,
+    up_hbm,
+    down_hbm,
+    sgate_hbm,
+    sup_hbm,
+    sdown_hbm,
+    out_ref,
     hx_ref,
     kt_all,
     v_all,
@@ -71,11 +85,68 @@
     acc,
     mstate,
     o_tok,
+    residual,
+    gate,
+    up,
+    down,
+    sgate,
+    sup,
+    sdown,
+    hidden,
+    shared,
+    meta,
+    place,
+    mixw,
+    nbx,
+    nby,
+    nbz,
+    sendx,
+    sendy,
+    sendz,
+    gotx,
+    goty,
+    gotz,
+    backx,
+    backy,
+    backz,
+    finx,
+    finy,
+    finz,
+    gsum,
+    hsum,
     send_sem,
     krecv,
     vrecv,
     xrecv,
+    load_sem,
+    ring_send,
+    ring_recv,
+    plane_send,
+    plane_recv,
 ):
+    near = (nbx, nby, nbz)
+    sending = (sendx, sendy, sendz)
+    got = (gotx, goty, gotz)
+    back = (backx, backy, backz)
+    fin = (finx, finy, finz)
+    loads = [
+        pltpu.make_async_copy(src, dst, load_sem.at[i])
+        for i, (src, dst) in enumerate(
+            (
+                (residual_hbm, residual),
+                (gate_hbm.at[0], gate),
+                (up_hbm.at[0], up),
+                (down_hbm.at[0], down),
+                (sgate_hbm, sgate),
+                (sup_hbm, sup),
+                (sdown_hbm, sdown),
+            )
+        )
+    ]
+    for d, (lo, hi) in enumerate(COLS):
+        for half, dst in enumerate((back[d], sending[d])):
+            src = out_proj_hbm.at[pl.ds(half * 32, 32), :, lo:hi]
+            loads.append(pltpu.make_async_copy(src, dst, load_sem.at[7 + 2 * d + half]))
     sp = lax.axis_index("sp")
     tx = lax.axis_index("tp")
     core = sp % 2
@@ -89,13 +160,33 @@
     y_next, y_prev = at(yy + 1, zz, core), at(yy + 3, zz, core)
     z_next, z_prev = at(yy, zz + 1, core), at(yy, zz + 3, core)
 
+    mine = (tx, yy, zz)
+    place_of = (sp, zz * 8 + core * 4 + tx, yy * 8 + core * 4 + tx)
+
+    def plane_device(d, q):
+        if d == 0:
+            return (q, tx)
+        c, x = (q // 4) % 2, q % 4
+        if d == 1:
+            return ((q // 8) * 8 + yy * 2 + c, x)
+        return (zz * 8 + (q // 8) * 2 + c, x)
+
+    def ring_device(d, j):
+        if d == 0:
+            return (sp, j)
+        if d == 1:
+            return (at(j, zz, core), tx)
+        return (at(yy, j, core), tx)
+
     barrier = pltpu.get_barrier_semaphore()
-    for peer in (sib, y_next, y_prev, z_next, z_prev):
-        pl.semaphore_signal(barrier, inc=1, device_id=(peer, tx), device_id_type=MESH)
-    for step in (1, 2, 3):
-        pl.semaphore_signal(
-            barrier, inc=1, device_id=(sp, (tx + step) % 4), device_id_type=MESH
-        )
+    for d in range(3):
+
+        def greet(i, carry, d=d):
+            peer = plane_device(d, (place_of[d] + i) % 32)
+            pl.semaphore_signal(barrier, inc=1, device_id=peer, device_id_type=MESH)
+            return carry
+
+        lax.fori_loop(1, 32, greet, 0)
 
     counter = [0]
     sent = []
@@ -136,12 +227,59 @@
     kr = normed_rotary(k_ref[...], kg_ref[...], trig[0], trig[1])
     kt_all[sp] = kr.T.astype(BF16)
     v_all[sp] = v_ref[...]
-    pl.semaphore_wait(barrier, 8)
+    pl.semaphore_wait(barrier, 93)
     for kind in (0, 1):
         for peer in (y_next, y_prev, z_next, z_prev):
             push(kind, sp, peer)
     push(0, sp, sib)
     push(1, sp, sib)
+    for load in loads:
+        load.start()
+
+    lane = lax.broadcasted_iota(jnp.int32, (128, 128), 1)
+    sub = lax.broadcasted_iota(jnp.int32, (128, 128), 0)
+    named = [routes_ref[:, k : k + 1] for k in range(4)]
+    hot = [(named[k] == lane).astype(F32) for k in range(4)]
+    every = (hot[0] + hot[1] + hot[2] + hot[3]).astype(BF16)
+    before = jnp.dot((lane < sub).astype(BF16), every, preferred_element_type=F32)
+    table = jnp.zeros((128, 128), F32)
+    for k in range(4):
+        rank = jnp.sum(hot[k] * before, axis=1, keepdims=True)
+        table = jnp.where(lane == k, named[k].astype(F32) * 8.0 + rank, table)
+        table = jnp.where(lane == 4 + k, rweight_ref[:, k : k + 1], table)
+    table = table.T[0:8, :]
+    for d in range(3):
+        meta[d, mine[d]] = table
+
+    def ring_copy(buf, dst, d, i, phase):
+        j = (mine[d] + i) % 4
+        if dst is None:
+            source, target = buf.at[mine[d]], buf.at[mine[d]]
+        else:
+            source, target = buf.at[j], dst.at[mine[d]]
+        return pltpu.make_async_remote_copy(
+            src_ref=source,
+            dst_ref=target,
+            send_sem=ring_send.at[phase, d, i],
+            recv_sem=ring_recv.at[phase, d, mine[d]],
+            device_id=ring_device(d, j),
+            device_id_type=MESH,
+        )
+
+    def ring_arrived(buf, d, i, phase):
+        j = (mine[d] + i) % 4
+        pltpu.make_async_remote_copy(
+            src_ref=buf.at[j],
+            dst_ref=buf.at[j],
+            send_sem=ring_send.at[phase, d, i],
+            recv_sem=ring_recv.at[phase, d, j],
+            device_id=ring_device(d, j),
+            device_id_type=MESH,
+        ).wait_recv()
+
+    for d in range(3):
+        for i in (1, 2, 3):
+            ring_copy(meta.at[d], None, d, i, 0).start()
 
     factor = math.log2(math.e) / math.sqrt(HD)
     for h in range(4):
@@ -300,6 +438,36 @@
         copy.start()
         exchanges.append(copy)
     hx_ref[tx] = o_tok[tx]
+    for d in range(3):
+        for i in (1, 2, 3):
+            ring_arrived(meta.at[d], d, i, 0)
+
+    def expert_of(d, q):
+        if d == 0:
+            return q * 4 + tx
+        c, x = (q >> 2) & 1, q & 3
+        if d == 1:
+            return ((q >> 3) * 8 + yy * 2 + c) * 4 + x
+        return (zz * 8 + (q >> 3) * 2 + c) * 4 + x
+
+    def wanted(d, r):
+        return (expert_of(d, r >> 4) * 8 + (r & 7) + ((r >> 3) & 1) * 4096).astype(F32)
+
+    for d in range(3):
+        want = wanted(d, lax.broadcasted_iota(jnp.int32, (512, 256), 0))
+        for pair in range(2):
+            first, second = meta[d, 2 * pair], meta[d, 2 * pair + 1]
+            hit = None
+            for k in range(4):
+                have = jnp.concatenate(
+                    [first[k : k + 1, :], second[k : k + 1, :] + 4096.0], axis=1
+                )
+                one = want == have
+                hit = one if hit is None else hit | one
+            place[d, pair] = jnp.where(hit, 1.0, 0.0).astype(BF16)
+    loads[0].wait()
+    for load in loads[7:]:
+        load.wait()
     for step in (1, 2, 3):
         source = (tx + step) % 4
         pltpu.make_async_remote_copy(
@@ -323,16 +491,184 @@
             device_id_type=MESH,
         ).wait_send()
 
-
-def attention(queries, keys, values, query_gain, key_gain):
+    heads = jnp.concatenate([hx_ref[j] for j in range(4)], axis=1)
+    square = jnp.zeros((128, 128), F32)
+    for d in range(3):
+        lo, hi = COLS[d]
+        weight = jnp.concatenate(
+            [back[d][...].reshape(1024, hi - lo), sending[d][...].reshape(1024, hi - lo)], axis=0
+        )
+        part = jnp.dot(heads, weight, preferred_element_type=F32)
+        h1 = (residual[:, lo:hi].astype(F32) + part).astype(BF16)
+        hidden[:, lo:hi] = h1
+        hf = h1.astype(F32)
+        hf = hf * hf
+        for j in range((hi - lo) // 128):
+            square = square + hf[:, j * 128 : (j + 1) * 128]
+    scale = lax.rsqrt(jnp.sum(square, axis=1, keepdims=True) * (1.0 / 2048.0) + EPS)
+    for d in range(3):
+        lo, hi = COLS[d]
+        near[d][mine[d]] = (hidden[:, lo:hi].astype(F32) * scale * ng_ref[:, lo:hi]).astype(BF16)
+        for i in (1, 2, 3):
+            ring_copy(near[d], None, d, i, 1).start()
+
+    def plane_copy(d, i, phase):
+        q = (place_of[d] + i) % 32
+        return pltpu.make_async_remote_copy(
+            src_ref=sending[d].at[q],
+            dst_ref=(got, back)[phase][d].at[place_of[d]],
+            send_sem=plane_send.at[phase, d, i],
+            recv_sem=plane_recv.at[phase, d, place_of[d]],
+            device_id=plane_device(d, q),
+            device_id_type=MESH,
+        )
+
+    def plane_arrived(d, q, phase):
+        buf = (got, back)[phase][d]
+
+        @pl.when(q != place_of[d])
+        def _():
+            pltpu.make_async_remote_copy(
+                src_ref=buf.at[q],
+                dst_ref=buf.at[q],
+                send_sem=plane_send.at[phase, d, 0],
+                recv_sem=plane_recv.at[phase, d, q],
+                device_id=plane_device(d, (place_of[d] + 1) % 32),
+                device_id_type=MESH,
+            ).wait_recv()
+
+    def each(lo, hi, act):
+        def go(i, carry):
+            act(i)
+            return carry
+
+        lax.fori_loop(lo, hi, go, 0)
+
+    for d in range(3):
+        width = COLS[d][1] - COLS[d][0]
+        for i in (1, 2, 3):
+            ring_arrived(near[d], d, i, 1)
+        for pair in range(2):
+            rows = near[d][2 * pair : 2 * pair + 2].reshape(256, width)
+            moved = jnp.dot(place[d, pair], rows, preferred_element_type=F32).astype(BF16)
+            sending[d][:, pair * 16 : (pair + 1) * 16, :] = moved.reshape(32, 16, width)
+        each(1, 32, lambda i, d=d: plane_copy(d, i, 0).start())
+        got[d][place_of[d]] = sending[d][place_of[d]]
+
+    for load in loads[1:7]:
+        load.wait()
+    gpart = jnp.zeros((128, 256), F32)
+    upart = jnp.zeros((128, 256), F32)
+    for d in range(3):
+        lo, hi = COLS[d]
+        rows = near[d][mine[d]]
+        gpart = gpart + jnp.dot(rows, sgate[lo:hi, :], preferred_element_type=F32)
+        upart = upart + jnp.dot(rows, sup[lo:hi, :], preferred_element_type=F32)
+    shid = (jax.nn.silu(gpart) * upart).astype(BF16)
+    for cb in range(4):
+        sl = slice(cb * 512, (cb + 1) * 512)
+        shared[:, sl] = jnp.dot(shid, sdown[:, sl], preferred_element_type=F32)
+
+    def block_of(d, q, j):
+        if d == 0:
+            return q * 4 + j
+        c, x = (q // 4) % 2, q % 4
+        if d == 1:
+            return (q // 8) * 32 + j * 8 + c * 4 + x
+        return j * 32 + (q // 8) * 8 + c * 4 + x
+
+    for g in range(4):
+        for d in range(3):
+            lo, hi = COLS[d]
+            each(g * 8, g * 8 + 8, lambda q, d=d: plane_arrived(d, q, 0))
+            rows = got[d][g * 8 : g * 8 + 8].reshape(256, hi - lo)
+            for n, weight in enumerate((gate, up)):
+                part = jnp.dot(rows, weight[lo:hi, :], preferred_element_type=F32)
+                for qi in range(8):
+                    for j in range(4):
+                        at_row = (qi * 4 + j) * 8
+                        b = block_of(d, g * 8 + qi, j)
+                        piece = part[at_row : at_row + 8, :]
+                        if d == 0:
+                            gsum[0, n, b] = piece
+                        elif d == 1:
+                            gsum[0, n, b] = gsum[0, n, b] + piece
+                        else:
+                            gsum[1, n, b] = piece
+    for z in range(4):
+        sl = slice(z * 32, (z + 1) * 32)
+        gg = (gsum[0, 0, sl] + gsum[1, 0, sl]).reshape(256, 256)
+        uu = (gsum[0, 1, sl] + gsum[1, 1, sl]).reshape(256, 256)
+        hsum[sl] = (jax.nn.silu(gg) * uu).reshape(32, 8, 256)
+    for d in range(3):
+        each(1, 32, lambda i, d=d: plane_copy(d, i, 0).wait_send())
+    for d in range(3):
+        lo, hi = COLS[d]
+        for g in range(4):
+            rows = jnp.concatenate(
+                [hsum[block_of(d, g * 8 + qi, j)] for qi in range(8) for j in range(4)], axis=0
+            ).astype(BF16)
+            result = jnp.dot(rows, down[:, lo:hi], preferred_element_type=F32).astype(BF16)
+            sending[d][g * 8 : g * 8 + 8] = result.reshape(8, 32, hi - lo)
+        each(1, 32, lambda i, d=d: plane_copy(d, i, 1).start())
+        back[d][place_of[d]] = sending[d][place_of[d]]
+
+    for d in range(3):
+        for i in (1, 2, 3):
+            ring_copy(near[d], None, d, i, 1).wait_send()
+            ring_copy(meta.at[d], None, d, i, 0).wait_send()
+    for d in range(3):
+        want = wanted(d, lax.broadcasted_iota(jnp.int32, (256, 512), 1))
+        for pair in range(2):
+            both = jnp.concatenate([meta[d, 2 * pair], meta[d, 2 * pair + 1]], axis=1)
+            tall = jnp.concatenate([both, jnp.zeros((120, 256), F32)], axis=0).T
+            shift = (lax.broadcasted_iota(jnp.int32, (256, 1), 0) >> 7).astype(F32) * 4096.0
+            total = jnp.zeros((256, 512), F32)
+            for k in range(4):
+                total = jnp.where(
+                    want == tall[:, k : k + 1] + shift, tall[:, 4 + k : 5 + k], total
+                )
+            total = total.astype(BF16)
+            mixw[d, pair] = total
+
+    for d in range(3):
+        lo, hi = COLS[d]
+        width = hi - lo
+        each(0, 32, lambda q, d=d: plane_arrived(d, q, 1))
+        for pair in range(2):
+            rows = back[d][:, pair * 16 : (pair + 1) * 16, :].reshape(512, width)
+            part = jnp.dot(mixw[d, pair], rows, preferred_element_type=F32).astype(BF16)
+            near[d][2 * pair : 2 * pair + 2] = part.reshape(2, 128, width)
+        for i in (1, 2, 3):
+            ring_copy(near[d], fin[d], d, i, 2).start()
+        fin[d][mine[d]] = near[d][mine[d]]
+    for d in range(3):
+        lo, hi = COLS[d]
+        for i in (1, 2, 3):
+            ring_arrived(fin[d], d, i, 2)
+        total = hidden[:, lo:hi].astype(F32) + shared[:, lo:hi]
+        for j in range(4):
+            total = total + fin[d][j].astype(F32)
+        out_ref[:, lo:hi] = total.astype(BF16)
+    for d in range(3):
+        for i in (1, 2, 3):
+            ring_copy(near[d], fin[d], d, i, 2).wait_send()
+        each(1, 32, lambda i, d=d: plane_copy(d, i, 1).wait_send())
+
+
+def layer(*operands):
     rows, cols = rotary_tables()
     vmem = pl.BlockSpec(memory_space=pltpu.VMEM)
+    hbm = pl.BlockSpec(memory_space=pl.ANY)
+    widths = [hi - lo for lo, hi in COLS]
+    weight = pltpu.VMEM((2048, 256), BF16)
     return pl.pallas_call(
-        attention_kernel,
-        out_shape=jax.ShapeDtypeStruct((4, 128, 512), BF16),
-        in_specs=[vmem] * 7,
+        layer_kernel,
+        out_shape=jax.ShapeDtypeStruct((128, 2048), BF16),
+        in_specs=[vmem] * 10 + [hbm] * 8,
         out_specs=vmem,
         scratch_shapes=[
+            pltpu.VMEM((4, 128, 512), BF16),
             pltpu.VMEM((32, HD, TOK), BF16),
             pltpu.VMEM((32, TOK, HD), BF16),
             pltpu.VMEM((4 * TOK, 2 * HD), BF16),
@@ -340,35 +676,40 @@
             pltpu.VMEM((4 * TOK, 2 * HD), F32),
             pltpu.VMEM((4 * TOK, HD), F32),
             pltpu.VMEM((4, 128, 4 * HD), BF16),
+            pltpu.VMEM((128, 2048), BF16),
+            weight,
+            weight,
+            pltpu.VMEM((256, 2048), BF16),
+            weight,
+            weight,
+            pltpu.VMEM((256, 2048), BF16),
+            pltpu.VMEM((128, 2048), BF16),
+            pltpu.VMEM((128, 2048), F32),
+            pltpu.VMEM((3, 4, 8, 128), F32),
+            pltpu.VMEM((3, 2, 512, 256), BF16),
+            pltpu.VMEM((3, 2, 256, 512), BF16),
+        ]
+        + [pltpu.VMEM((4, 128, w), BF16) for w in widths]
+        + [pltpu.VMEM((32, 32, w), BF16) for w in widths * 3]
+        + [pltpu.VMEM((4, 128, w), BF16) for w in widths]
+        + [
+            pltpu.VMEM((2, 2, 128, 8, 256), F32),
+            pltpu.VMEM((128, 8, 256), F32),
             pltpu.SemaphoreType.DMA((72,)),
             pltpu.SemaphoreType.DMA((32,)),
             pltpu.SemaphoreType.DMA((32,)),
             pltpu.SemaphoreType.DMA((4,)),
+            pltpu.SemaphoreType.DMA((13,)),
+            pltpu.SemaphoreType.DMA((3, 3, 4)),
+            pltpu.SemaphoreType.DMA((3, 3, 4)),
+            pltpu.SemaphoreType.DMA((2, 3, 32)),
+            pltpu.SemaphoreType.DMA((2, 3, 32)),
         ],
         compiler_params=pltpu.CompilerParams(
-            collective_id=0, has_side_effects=True, vmem_limit_bytes=56 * 2**20
+            collective_id=0, has_side_effects=True, vmem_limit_bytes=67043328
         ),
-        name="attention",
-    )(
-        queries,
-        keys,
-        values,
-        query_gain.reshape(1, HD),
-        key_gain.reshape(1, HD),
-        jnp.asarray(rows),
-        jnp.asarray(cols),
-    )
-
-
-def expert_apply(arrived, expert_gate, expert_up, expert_down):
-    sources, slots, width = arrived.shape
-    local = expert_gate.shape[0]
-    grouped = arrived.reshape(sources // local, local, slots, width)
-    gate_part = jnp.einsum("sech,ehf->secf", grouped, expert_gate, preferred_element_type=F32)
-    up_part = jnp.einsum("sech,ehf->secf", grouped, expert_up, preferred_element_type=F32)
-    hidden_e = (jax.nn.silu(gate_part) * up_part).astype(BF16)
-    result = jnp.einsum("secf,efh->sech", hidden_e, expert_down, preferred_element_type=F32)
-    return result.astype(BF16).reshape(sources, slots, width)
+        name="layer",
+    )(*operands[:5], jnp.asarray(rows), jnp.asarray(cols), *operands[5:])
 
 
 def body(
@@ -389,52 +730,24 @@
     shared_up,
     shared_down,
 ):
-    heads_x = attention(queries, keys, values, query_gain, key_gain)
-    all_heads = heads_x.transpose(1, 0, 2).reshape(128, 2048)
-    projected = jnp.dot(all_heads, out_proj, preferred_element_type=F32)
-    hidden1 = (residual.astype(F32) + projected).astype(BF16)
-    hidden_f = hidden1.astype(F32)
-    normed = (
-        hidden_f
-        * lax.rsqrt(jnp.mean(hidden_f * hidden_f, axis=-1, keepdims=True) + EPS)
-        * norm_gain
-    ).astype(BF16)
-    rows_local = normed.shape[0]
-    top_count = routes.shape[1]
-    pair_count = rows_local * top_count
-    expert_total = expert_gate.shape[0] * lax.axis_size("sp") * lax.axis_size("tp")
-    capacity = 8
-    flat_routes = routes.reshape(pair_count)
-    one_hot = (flat_routes[:, None] == jnp.arange(expert_total, dtype=jnp.int32)[None, :]).astype(
-        F32
-    )
-    lower = (jnp.arange(pair_count)[:, None] >= jnp.arange(pair_count)[None, :]).astype(F32)
-    running_count = jnp.dot(lower, one_hot, precision=lax.Precision.HIGHEST)
-    slot_place = (jnp.sum(running_count * one_hot, axis=1) - 1.0).astype(jnp.int32)
-    slot_index = flat_routes * capacity + slot_place
-    slot_total = expert_total * capacity
-    placement = (jnp.arange(slot_total, dtype=jnp.int32)[:, None] == slot_index[None, :]).astype(
-        BF16
-    )
-    placement = jnp.sum(placement.reshape(slot_total, rows_local, top_count), axis=2)
-    send_rows = jnp.dot(placement, normed, preferred_element_type=F32).astype(BF16)
-    send_rows = send_rows.reshape(expert_total, capacity, normed.shape[1])
-    shared_hidden = (
-        jax.nn.silu(jnp.dot(normed, shared_gate, preferred_element_type=F32))
-        * jnp.dot(normed, shared_up, preferred_element_type=F32)
-    ).astype(BF16)
-    shared_out = jnp.dot(shared_hidden, shared_down, preferred_element_type=F32)
-    processed = expert_apply(
-        lax.all_to_all(send_rows, ("sp", "tp"), split_axis=0, concat_axis=0, tiled=True),
+    return layer(
+        queries,
+        keys,
+        values,
+        query_gain.reshape(1, HD),
+        key_gain.reshape(1, HD),
+        norm_gain.reshape(1, 2048),
+        routes,
+        route_weight,
+        residual,
+        out_proj.reshape(64, 32, 2048),
         expert_gate,
         expert_up,
         expert_down,
+        shared_gate,
+        shared_up,
+        shared_down,
     )
-    returned = lax.all_to_all(processed, ("sp", "tp"), split_axis=0, concat_axis=0, tiled=True)
-    returned = returned.reshape(slot_total, normed.shape[1])
-    routed = returned[slot_index].reshape(rows_local, top_count, normed.shape[1]).astype(F32)
-    mixed = jnp.einsum("tk,tkd->td", route_weight, routed) + shared_out
-    return (hidden_f + mixed).astype(BF16)
 
 
 def solution(mesh):

time: 219 us -> 194 us (0.89)
  Pallas kernels: 62.7 us -> 187 us
  blocking collectives: 60.8 us -> 0 us
  waiting for transfers between devices: 52.5 us -> 0 us
  matrix products: 17.6 us -> 0 us
  local copies, waits for them, and re-layouts: 19.2 us -> 4.7 us
  starting transfers between devices: 5.18 us -> 0 us
    pallas_call x1, Pallas kernels: 62.7 us -> 187 us  [layer(): pl.pallas_call(layer_kernel, out_shape=jax.ShapeDtypeStruct((128, 2048),...]
    all_to_all x1 -> x0, blocking collectives: 60.8 us -> none  [body(): lax.all_to_all(send_rows, ('sp', 'tp'), split_axis=0, concat_axis=0, tile...]
    all_to_all x1 -> x0, waiting for transfers between devices: 52.5 us -> none  [body(): lax.all_to_all(processed, ('sp', 'tp'), split_axis=0, concat_axis=0, tile...]
    dot_general x9 -> x0, matrix products: 17.6 us -> none  [the longest x1 4.74 us: body(): projected = jnp.dot(all_heads, out_proj, preferred_element_type=F32)]
    gather x1 -> x0, local copies, waits for them, and re-layouts: 7.98 us -> none  [body(): returned[slot_index].reshape(rows_local, top_count, normed.shape[1])]
    all_to_all x1 -> x0, starting transfers between devices: 5.18 us -> none  [body(): lax.all_to_all(processed, ('sp', 'tp'), split_axis=0, concat_axis=0, tile...]
    convert_element_type x2 -> x0, local copies, waits for them, and re-layouts: 4.37 us -> none  [the longest x1 4.27 us: expert_apply(): return result.astype(BF16).reshape(sources, slots, width)]
    reshape x1 -> x0, local copies, waits for them, and re-layouts: 4.17 us -> none  [body(): returned[slot_index].reshape(rows_local, top_count, normed.shape[1])]
  transfers between devices with their start and end apart: 1 -> 0, of which waited for: 1 -> 0; matrix products, arithmetic and copies ran while one was open for 0% -> 0% of each run, Pallas kernels for 0% -> 0%
where the time goes in v2:
time: 194 us; the launch traced here: 191 us
  Pallas kernels  187 us (96%)
  local copies, waits for them, and re-layouts  4.7 us (2%)
    pallas_call x1, Pallas kernels, layer(): pl.pallas_call(layer_kernel, out_shape=jax.ShapeDtypeStruct((128, 2048),...  187 us
    unnamed x3, local copies, waits for them, and re-layouts  4.7 us

profile of v2, /device:TPU:1, one launch (start us, length us, event | category | flops | bytes accessed | tf_op | source)
XLA Modules:
  0.0 191.2 jit_solution(9977547282654779473)
XLA Ops:
  0.0 1.4 copy.19.routes_ref
  1.4 1.4 copy.20.rweight_ref
  2.8 186.5 %layer.1 = bf16[128,2048]{1,0:T(8,128)(2,1)} custom-call(bf16[512,512]{1,0:T(8,128)(2,1)} %q_ref.1, bf16[512,128]{1,0:T(8,128)(2,1)} %k_ref.1, bf16[512,128]{1,0:T(8,128)(2,1)} %v_ref.1, f32[1,128]{1,0:T(1,128)} %bitcast.6, f32[1,128]{1,0:T(1,128)} %bitcast.7, f32[2,256,128]{2,1,0:T(8,128)} %constant.4.clone.rows_ref, f32[2,64,128]{2,1,0:T(8,128)} %constant.5.clone.cols_ref, ...), custom_call_target="tpu_custom_call" | custom-call | tf_op jit(solution)/shard_map/layer/pallas_call | solution.py:665
  189.4 1.9 copy.22

commit v3 on v2

--- a/solution.py
+++ b/solution.py
@@ -54,6 +54,13 @@
 E_SET = ((2, 2),)
 
 
+def far(a):
+    return 2 if a == 2 else a % 2
+
+
+PLANE = [(a, b, c) for a in range(4) for b in range(4) for c in range(2) if a or b or c]
+FARTHEST = sorted(PLANE, key=lambda m: -far(m[0]) - far(m[1]))
+GROUPED = sorted(PLANE, key=lambda m: (-far(m[0]), -far(m[1]), m[2], m[1], m[0]))
 COLS = ((0, 640), (640, 1280), (1280, 2048))
 
 
@@ -95,6 +102,7 @@
     hidden,
     shared,
     meta,
+    table_s,
     place,
     mixw,
     nbx,
@@ -117,7 +125,8 @@
     send_sem,
     krecv,
     vrecv,
-    xrecv,
+    head_send,
+    head_recv,
     load_sem,
     ring_send,
     ring_recv,
@@ -179,14 +188,9 @@
         return (at(yy, j, core), tx)
 
     barrier = pltpu.get_barrier_semaphore()
-    for d in range(3):
-
-        def greet(i, carry, d=d):
-            peer = plane_device(d, (place_of[d] + i) % 32)
-            pl.semaphore_signal(barrier, inc=1, device_id=peer, device_id_type=MESH)
-            return carry
-
-        lax.fori_loop(1, 32, greet, 0)
+    peers = [(sib, tx)] + [ring_device(d, (mine[d] + i) % 4) for d in range(3) for i in (1, 2, 3)]
+    for peer in peers:
+        pl.semaphore_signal(barrier, inc=1, device_id=peer, device_id_type=MESH)
 
     counter = [0]
     sent = []
@@ -227,29 +231,15 @@
     kr = normed_rotary(k_ref[...], kg_ref[...], trig[0], trig[1])
     kt_all[sp] = kr.T.astype(BF16)
     v_all[sp] = v_ref[...]
-    pl.semaphore_wait(barrier, 93)
-    for kind in (0, 1):
-        for peer in (y_next, y_prev, z_next, z_prev):
-            push(kind, sp, peer)
-    push(0, sp, sib)
-    push(1, sp, sib)
-    for load in loads:
-        load.start()
-
-    lane = lax.broadcasted_iota(jnp.int32, (128, 128), 1)
-    sub = lax.broadcasted_iota(jnp.int32, (128, 128), 0)
-    named = [routes_ref[:, k : k + 1] for k in range(4)]
-    hot = [(named[k] == lane).astype(F32) for k in range(4)]
-    every = (hot[0] + hot[1] + hot[2] + hot[3]).astype(BF16)
-    before = jnp.dot((lane < sub).astype(BF16), every, preferred_element_type=F32)
-    table = jnp.zeros((128, 128), F32)
-    for k in range(4):
-        rank = jnp.sum(hot[k] * before, axis=1, keepdims=True)
-        table = jnp.where(lane == k, named[k].astype(F32) * 8.0 + rank, table)
-        table = jnp.where(lane == 4 + k, rweight_ref[:, k : k + 1], table)
-    table = table.T[0:8, :]
-    for d in range(3):
-        meta[d, mine[d]] = table
+    factor = math.log2(math.e) / math.sqrt(HD)
+    for h in range(4):
+        qr = normed_rotary(q_ref[:, h * HD : (h + 1) * HD], qg_ref[...], trig[0], trig[1])
+        qs = qr.astype(BF16).astype(F32) * factor
+        hi = qs.astype(BF16)
+        q_hl[h * TOK : (h + 1) * TOK, 0:HD] = hi
+        q_hl[h * TOK : (h + 1) * TOK, HD : 2 * HD] = (qs - hi.astype(F32)).astype(BF16)
+    acc[...] = jnp.zeros_like(acc)
+    mstate[...] = jnp.full_like(mstate, -1e30)
 
     def ring_copy(buf, dst, d, i, phase):
         j = (mine[d] + i) % 4
@@ -277,21 +267,39 @@
             device_id_type=MESH,
         ).wait_recv()
 
+    pl.semaphore_wait(barrier, 10)
+    for kind in (0, 1):
+        for peer in (y_next, y_prev, z_next, z_prev):
+            push(kind, sp, peer)
+    push(0, sp, sib)
+    push(1, sp, sib)
+    for load in loads:
+        load.start()
+
+    lane = lax.broadcasted_iota(jnp.int32, (128, 128), 1)
+    sub = lax.broadcasted_iota(jnp.int32, (128, 128), 0)
+    table_s[...] = jnp.zeros((128, 128), F32)
+    table_s[0:4, :] = routes_ref[...].astype(F32)
+    table_s[4:8, :] = rweight_ref[...]
+    tall = table_s[...].T
+    hot = [(tall[:, k : k + 1] == lane.astype(F32)).astype(F32) for k in range(4)]
+    every = (hot[0] + hot[1] + hot[2] + hot[3]).astype(BF16)
+    before = jnp.dot((lane < sub).astype(BF16), every, preferred_element_type=F32)
+    table = jnp.where(lane < 8, tall, 0.0)
+    for k in range(4):
+        rank = jnp.sum(hot[k] * before, axis=1, keepdims=True)
+        table = jnp.where(lane == k, tall[:, k : k + 1] * 8.0 + rank, table)
+    table = table.T[0:8, :]
+    for d in range(3):
+        meta[d, mine[d]] = table
     for d in range(3):
         for i in (1, 2, 3):
             ring_copy(meta.at[d], None, d, i, 0).start()
 
-    factor = math.log2(math.e) / math.sqrt(HD)
-    for h in range(4):
-        qr = normed_rotary(q_ref[:, h * HD : (h + 1) * HD], qg_ref[...], trig[0], trig[1])
-        qs = qr.astype(BF16).astype(F32) * factor
-        hi = qs.astype(BF16)
-        q_hl[h * TOK : (h + 1) * TOK, 0:HD] = hi
-        q_hl[h * TOK : (h + 1) * TOK, HD : 2 * HD] = (qs - hi.astype(F32)).astype(BF16)
-    acc[...] = jnp.zeros_like(acc)
-    mstate[...] = jnp.full_like(mstate, -1e30)
-
-    def attend(slots):
+    def head_rows(h):
+        return pl.ds(pl.multiple_of(h * TOK, TOK), TOK)
+
+    def attend(slots, heads=(0, 1, 2, 3)):
         n = len(slots)
         width = n * TOK
         kt = jnp.concatenate([kt_all[s] for s in slots], axis=1)
@@ -300,13 +308,11 @@
         v2 = jnp.concatenate([vv, jnp.ones_like(vv)], axis=1)
 
         def scores(h):
-            return jnp.dot(
-                q_hl[h * TOK : (h + 1) * TOK, :], k2, preferred_element_type=F32
-            )
-
-        s = scores(0)
-        for h in range(4):
-            sl = slice(h * TOK, (h + 1) * TOK)
+            return jnp.dot(q_hl[head_rows(h), :], k2, preferred_element_type=F32)
+
+        s = scores(heads[0])
+        for i, h in enumerate(heads):
+            sl = head_rows(h)
             old = mstate[sl, :]
             top = s[:, 0:HD]
             for j in range(1, width // HD):
@@ -314,8 +320,8 @@
             new = jnp.maximum(old, jnp.max(top, axis=1, keepdims=True))
             mstate[sl, :] = new
             p = jnp.exp2(s - new[:, 0:1]).astype(BF16)
-            if h < 3:
-                s = scores(h + 1)
+            if i + 1 < len(heads):
+                s = scores(heads[i + 1])
             shrink = jnp.exp2(old - new)
             pv = jnp.dot(p, v2, preferred_element_type=F32)
             acc[sl, :] = acc[sl, :] * jnp.concatenate([shrink, shrink], axis=1) + pv
@@ -334,6 +340,47 @@
     arrived(0, sib)
     arrived(1, sib)
     attend([sp, sib])
+
+    for d in range(3):
+        for i in (1, 2, 3):
+            ring_arrived(meta.at[d], d, i, 0)
+
+    def expert_of(d, q):
+        if d == 0:
+            return q * 4 + tx
+        c, x = (q >> 2) & 1, q & 3
+        if d == 1:
+            return ((q >> 3) * 8 + yy * 2 + c) * 4 + x
+        return (zz * 8 + (q >> 3) * 2 + c) * 4 + x
+
+    def wanted(d, r):
+        return (expert_of(d, r >> 4) * 8 + (r & 7) + ((r >> 3) & 1) * 4096).astype(F32)
+
+    for d in range(3):
+        want = wanted(d, lax.broadcasted_iota(jnp.int32, (512, 256), 0))
+        for pair in range(2):
+            first, second = meta[d, 2 * pair], meta[d, 2 * pair + 1]
+            hit = None
+            for k in range(4):
+                have = jnp.concatenate(
+                    [first[k : k + 1, :], second[k : k + 1, :] + 4096.0], axis=1
+                )
+                one = want == have
+                hit = one if hit is None else hit | one
+            place[d, pair] = jnp.where(hit, 1.0, 0.0).astype(BF16)
+    for d in range(3):
+        want = wanted(d, lax.broadcasted_iota(jnp.int32, (256, 512), 1))
+        for pair in range(2):
+            both = jnp.concatenate([meta[d, 2 * pair], meta[d, 2 * pair + 1]], axis=1)
+            tall = jnp.concatenate([both, jnp.zeros((120, 256), F32)], axis=0).T
+            shift = (lax.broadcasted_iota(jnp.int32, (256, 1), 0) >> 7).astype(F32) * 4096.0
+            total = jnp.zeros((256, 512), F32)
+            for k in range(4):
+                total = jnp.where(
+                    want == tall[:, k : k + 1] + shift, tall[:, 4 + k : 5 + k], total
+                )
+            total = total.astype(BF16)
+            mixw[d, pair] = total
 
     def event(t):
         if t == 0:
@@ -414,72 +461,47 @@
         attend(slots)
         return carry
 
-    lax.fori_loop(0, 7, one_step, 0)
+    lax.fori_loop(0, 6, one_step, 0)
+    event(6)
     pair_arrived(2, 2, 1 - core)
-    attend([origin(2, 2, core), origin(2, 2, 1 - core)])
-
-    for h in range(4):
-        sl = slice(h * TOK, (h + 1) * TOK)
-        o = (acc[sl, 0:HD] / acc[sl, HD : 2 * HD]).astype(BF16)
-        for j in range(4):
-            o_tok[j, :, h * HD : (h + 1) * HD] = o[j * 128 : (j + 1) * 128, :]
-    exchanges = []
-    for step in (1, 2, 3):
+    late = [origin(dy, dz, 1 - core) for dy, dz in D_SET]
+    last = [origin(2, 2, core), origin(2, 2, 1 - core)]
+
+    def head_copy(step, h, source):
         peer = (tx + step) % 4
-        copy = pltpu.make_async_remote_copy(
-            src_ref=o_tok.at[peer],
-            dst_ref=hx_ref.at[tx],
-            send_sem=send_sem.at[counter[0]],
-            recv_sem=xrecv.at[tx],
+        return pltpu.make_async_remote_copy(
+            src_ref=o_tok.at[peer, h],
+            dst_ref=hx_ref.at[source, h],
+            send_sem=head_send.at[step, h],
+            recv_sem=head_recv.at[source, h],
             device_id=(sp, peer),
             device_id_type=MESH,
         )
-        counter[0] += 1
-        copy.start()
-        exchanges.append(copy)
-    hx_ref[tx] = o_tok[tx]
-    for d in range(3):
-        for i in (1, 2, 3):
-            ring_arrived(meta.at[d], d, i, 0)
-
-    def expert_of(d, q):
-        if d == 0:
-            return q * 4 + tx
-        c, x = (q >> 2) & 1, q & 3
-        if d == 1:
-            return ((q >> 3) * 8 + yy * 2 + c) * 4 + x
-        return (zz * 8 + (q >> 3) * 2 + c) * 4 + x
-
-    def wanted(d, r):
-        return (expert_of(d, r >> 4) * 8 + (r & 7) + ((r >> 3) & 1) * 4096).astype(F32)
-
-    for d in range(3):
-        want = wanted(d, lax.broadcasted_iota(jnp.int32, (512, 256), 0))
-        for pair in range(2):
-            first, second = meta[d, 2 * pair], meta[d, 2 * pair + 1]
-            hit = None
-            for k in range(4):
-                have = jnp.concatenate(
-                    [first[k : k + 1, :], second[k : k + 1, :] + 4096.0], axis=1
-                )
-                one = want == have
-                hit = one if hit is None else hit | one
-            place[d, pair] = jnp.where(hit, 1.0, 0.0).astype(BF16)
+
+    def finish(pair, carry):
+        heads = (2 * pair, 2 * pair + 1)
+        attend(late, heads)
+        attend(last, heads)
+        for h in heads:
+            a = acc[head_rows(h), :]
+            o = (a[:, 0:HD] / a[:, HD : 2 * HD]).astype(BF16)
+            for j in range(4):
+                o_tok[j, h] = o[j * 128 : (j + 1) * 128, :]
+            for step in (1, 2, 3):
+                head_copy(step, h, tx).start()
+            hx_ref[tx, h] = o_tok[tx, h]
+        return carry
+
+    lax.fori_loop(0, 2, finish, 0)
     loads[0].wait()
     for load in loads[7:]:
         load.wait()
-    for step in (1, 2, 3):
-        source = (tx + step) % 4
-        pltpu.make_async_remote_copy(
-            src_ref=o_tok.at[source],
-            dst_ref=hx_ref.at[source],
-            send_sem=send_sem.at[0],
-            recv_sem=xrecv.at[source],
-            device_id=(sp, source),
-            device_id_type=MESH,
-        ).wait_recv()
-    for copy in exchanges:
-        copy.wait_send()
+    for h in range(4):
+        for step in (1, 2, 3):
+            head_copy(step, h, (tx + step) % 4).wait_recv()
+    for h in range(4):
+        for step in (1, 2, 3):
+            head_copy(step, h, tx).wait_send()
     for kind, index in sent:
         buf, recv = (kt_all, krecv) if kind == 0 else (v_all, vrecv)
         pltpu.make_async_remote_copy(
@@ -491,7 +513,7 @@
             device_id_type=MESH,
         ).wait_send()
 
-    heads = jnp.concatenate([hx_ref[j] for j in range(4)], axis=1)
+    heads = jnp.concatenate([hx_ref[j, h] for j in range(4) for h in range(4)], axis=1)
     square = jnp.zeros((128, 128), F32)
     for d in range(3):
         lo, hi = COLS[d]
@@ -512,8 +534,7 @@
         for i in (1, 2, 3):
             ring_copy(near[d], None, d, i, 1).start()
 
-    def plane_copy(d, i, phase):
-        q = (place_of[d] + i) % 32
+    def plane_copy(d, q, i, phase):
         return pltpu.make_async_remote_copy(
             src_ref=sending[d].at[q],
             dst_ref=(got, back)[phase][d].at[place_of[d]],
@@ -522,6 +543,22 @@
             device_id=plane_device(d, q),
             device_id_type=MESH,
         )
+
+    def spray(order, phase):
+        for i, (da, db, dc) in enumerate(order):
+            c = (core + dc) % 2
+            plane_copy(0, ((zz + da) % 4) * 8 + ((yy + db) % 4) * 2 + c, i, phase).start()
+            plane_copy(1, ((zz + da) % 4) * 8 + c * 4 + (tx + db) % 4, i, phase).start()
+            plane_copy(2, ((yy + da) % 4) * 8 + c * 4 + (tx + db) % 4, i, phase).start()
+
+    def sprayed(phase):
+        for d in range(3):
+
+            def go(i, carry, d=d):
+                plane_copy(d, (place_of[d] + 1) % 32, i, phase).wait_send()
+                return carry
+
+            lax.fori_loop(0, 31, go, 0)
 
     def plane_arrived(d, q, phase):
         buf = (got, back)[phase][d]
@@ -552,8 +589,8 @@
             rows = near[d][2 * pair : 2 * pair + 2].reshape(256, width)
             moved = jnp.dot(place[d, pair], rows, preferred_element_type=F32).astype(BF16)
             sending[d][:, pair * 16 : (pair + 1) * 16, :] = moved.reshape(32, 16, width)
-        each(1, 32, lambda i, d=d: plane_copy(d, i, 0).start())
         got[d][place_of[d]] = sending[d][place_of[d]]
+    spray(GROUPED, 0)
 
     for load in loads[1:7]:
         load.wait()
@@ -569,25 +606,26 @@
         sl = slice(cb * 512, (cb + 1) * 512)
         shared[:, sl] = jnp.dot(shid, sdown[:, sl], preferred_element_type=F32)
 
-    def block_of(d, q, j):
+    def block_of(d, g, qi, j):
         if d == 0:
-            return q * 4 + j
-        c, x = (q // 4) % 2, q % 4
+            return g * 32 + qi * 4 + j
+        c, x = qi // 4, qi % 4
         if d == 1:
-            return (q // 8) * 32 + j * 8 + c * 4 + x
-        return j * 32 + (q // 8) * 8 + c * 4 + x
-
-    for g in range(4):
+            return g * 32 + j * 8 + c * 4 + x
+        return j * 32 + g * 8 + c * 4 + x
+
+    for step in (2, 1, 3, 0):
         for d in range(3):
             lo, hi = COLS[d]
-            each(g * 8, g * 8 + 8, lambda q, d=d: plane_arrived(d, q, 0))
-            rows = got[d][g * 8 : g * 8 + 8].reshape(256, hi - lo)
+            g = ((zz, zz, yy)[d] + step) % 4
+            each(0, 8, lambda q, d=d, g=g: plane_arrived(d, g * 8 + q, 0))
+            rows = got[d][pl.ds(g * 8, 8)].reshape(256, hi - lo)
             for n, weight in enumerate((gate, up)):
                 part = jnp.dot(rows, weight[lo:hi, :], preferred_element_type=F32)
                 for qi in range(8):
                     for j in range(4):
                         at_row = (qi * 4 + j) * 8
-                        b = block_of(d, g * 8 + qi, j)
+                        b = block_of(d, g, qi, j)
                         piece = part[at_row : at_row + 8, :]
                         if d == 0:
                             gsum[0, n, b] = piece
@@ -600,37 +638,22 @@
         gg = (gsum[0, 0, sl] + gsum[1, 0, sl]).reshape(256, 256)
         uu = (gsum[0, 1, sl] + gsum[1, 1, sl]).reshape(256, 256)
         hsum[sl] = (jax.nn.silu(gg) * uu).reshape(32, 8, 256)
-    for d in range(3):
-        each(1, 32, lambda i, d=d: plane_copy(d, i, 0).wait_send())
+    sprayed(0)
     for d in range(3):
         lo, hi = COLS[d]
         for g in range(4):
             rows = jnp.concatenate(
-                [hsum[block_of(d, g * 8 + qi, j)] for qi in range(8) for j in range(4)], axis=0
+                [hsum[block_of(d, g, qi, j)] for qi in range(8) for j in range(4)], axis=0
             ).astype(BF16)
             result = jnp.dot(rows, down[:, lo:hi], preferred_element_type=F32).astype(BF16)
             sending[d][g * 8 : g * 8 + 8] = result.reshape(8, 32, hi - lo)
-        each(1, 32, lambda i, d=d: plane_copy(d, i, 1).start())
         back[d][place_of[d]] = sending[d][place_of[d]]
+    spray(FARTHEST, 1)
 
     for d in range(3):
         for i in (1, 2, 3):
             ring_copy(near[d], None, d, i, 1).wait_send()
             ring_copy(meta.at[d], None, d, i, 0).wait_send()
-    for d in range(3):
-        want = wanted(d, lax.broadcasted_iota(jnp.int32, (256, 512), 1))
-        for pair in range(2):
-            both = jnp.concatenate([meta[d, 2 * pair], meta[d, 2 * pair + 1]], axis=1)
-            tall = jnp.concatenate([both, jnp.zeros((120, 256), F32)], axis=0).T
-            shift = (lax.broadcasted_iota(jnp.int32, (256, 1), 0) >> 7).astype(F32) * 4096.0
-            total = jnp.zeros((256, 512), F32)
-            for k in range(4):
-                total = jnp.where(
-                    want == tall[:, k : k + 1] + shift, tall[:, 4 + k : 5 + k], total
-                )
-            total = total.astype(BF16)
-            mixw[d, pair] = total
-
     for d in range(3):
         lo, hi = COLS[d]
         width = hi - lo
@@ -653,7 +676,7 @@
     for d in range(3):
         for i in (1, 2, 3):
             ring_copy(near[d], fin[d], d, i, 2).wait_send()
-        each(1, 32, lambda i, d=d: plane_copy(d, i, 1).wait_send())
+    sprayed(1)
 
 
 def layer(*operands):
@@ -668,14 +691,14 @@
         in_specs=[vmem] * 10 + [hbm] * 8,
         out_specs=vmem,
         scratch_shapes=[
-            pltpu.VMEM((4, 128, 512), BF16),
+            pltpu.VMEM((4, 4, 128, HD), BF16),
             pltpu.VMEM((32, HD, TOK), BF16),
             pltpu.VMEM((32, TOK, HD), BF16),
             pltpu.VMEM((4 * TOK, 2 * HD), BF16),
             pltpu.VMEM((2, TOK, HD), F32),
             pltpu.VMEM((4 * TOK, 2 * HD), F32),
             pltpu.VMEM((4 * TOK, HD), F32),
-            pltpu.VMEM((4, 128, 4 * HD), BF16),
+            pltpu.VMEM((4, 4, 128, HD), BF16),
             pltpu.VMEM((128, 2048), BF16),
             weight,
             weight,
@@ -686,6 +709,7 @@
             pltpu.VMEM((128, 2048), BF16),
             pltpu.VMEM((128, 2048), F32),
             pltpu.VMEM((3, 4, 8, 128), F32),
+            pltpu.VMEM((128, 128), F32),
             pltpu.VMEM((3, 2, 512, 256), BF16),
             pltpu.VMEM((3, 2, 256, 512), BF16),
         ]
@@ -698,7 +722,8 @@
             pltpu.SemaphoreType.DMA((72,)),
             pltpu.SemaphoreType.DMA((32,)),
             pltpu.SemaphoreType.DMA((32,)),
-            pltpu.SemaphoreType.DMA((4,)),
+            pltpu.SemaphoreType.DMA((4, 4)),
+            pltpu.SemaphoreType.DMA((4, 4)),
             pltpu.SemaphoreType.DMA((13,)),
             pltpu.SemaphoreType.DMA((3, 3, 4)),
             pltpu.SemaphoreType.DMA((3, 3, 4)),
@@ -737,8 +762,8 @@
         query_gain.reshape(1, HD),
         key_gain.reshape(1, HD),
         norm_gain.reshape(1, 2048),
-        routes,
-        route_weight,
+        routes.T,
+        route_weight.T,
         residual,
         out_proj.reshape(64, 32, 2048),
         expert_gate,

time: 194 us -> 169 us (0.87); the launches traced: 191 us -> 169 us
  Pallas kernels: 187 us -> 167 us
  local copies, waits for them, and re-layouts: 4.7 us -> 1.88 us
    pallas_call x1, Pallas kernels: 187 us -> 167 us  [layer(): pl.pallas_call(layer_kernel, out_shape=jax.ShapeDtypeStruct((128, 2048),...]
    unnamed x3 -> x1, local copies, waits for them, and re-layouts: 4.7 us -> 1.88 us
where the time goes in v3:
time: 169 us
  Pallas kernels  167 us (99%)
  local copies, waits for them, and re-layouts  1.88 us (1%)
    pallas_call x1, Pallas kernels, layer(): pl.pallas_call(layer_kernel, out_shape=jax.ShapeDtypeStruct((128, 2048),...  167 us

profile of v3, /device:TPU:1, one launch (start us, length us, event | category | flops | bytes accessed | tf_op | source)
XLA Modules:
  0.0 168.9 jit_solution(15051406673022127020)
XLA Ops:
  0.0 167.0 %layer.1 = bf16[128,2048]{1,0:T(8,128)(2,1)} custom-call(bf16[512,512]{1,0:T(8,128)(2,1)} %q_ref.1, bf16[512,128]{1,0:T(8,128)(2,1)} %k_ref.1, bf16[512,128]{1,0:T(8,128)(2,1)} %v_ref.1, f32[1,128]{1,0:T(1,128)} %bitcast.10, f32[1,128]{1,0:T(1,128)} %bitcast.11, f32[2,256,128]{2,1,0:T(8,128)} %constant.4.clone.rows_ref, ...), custom_call_target="tpu_custom_call" | custom-call | tf_op jit(solution)/shard_map/layer/pallas_call | solution.py:688
  167.0 1.9 %copy.20 = bf16[128,2048]{1,0:T(8,128)(2,1)} copy(bf16[128,2048]{1,0:T(8,128)(2,1)} %layer.1) | data formatting | bytes 1048576

commit v4 on v3

--- a/solution.py
+++ b/solution.py
@@ -59,22 +59,21 @@
 
 
 PLANE = [(a, b, c) for a in range(4) for b in range(4) for c in range(2) if a or b or c]
-FARTHEST = sorted(PLANE, key=lambda m: -far(m[0]) - far(m[1]))
 GROUPED = sorted(PLANE, key=lambda m: (-far(m[0]), -far(m[1]), m[2], m[1], m[0]))
 COLS = ((0, 640), (640, 1280), (1280, 2048))
 
 
 def layer_kernel(
-    q_ref,
-    k_ref,
-    v_ref,
-    qg_ref,
-    kg_ref,
-    rows_ref,
-    cols_ref,
-    ng_ref,
-    routes_ref,
-    rweight_ref,
+    q_hbm,
+    k_hbm,
+    v_hbm,
+    qg_hbm,
+    kg_hbm,
+    rows_hbm,
+    cols_hbm,
+    ng_hbm,
+    routes_hbm,
+    rweight_hbm,
     residual_hbm,
     out_proj_hbm,
     gate_hbm,
@@ -84,6 +83,15 @@
     sup_hbm,
     sdown_hbm,
     out_ref,
+    q_ref,
+    k_ref,
+    qg_ref,
+    kg_ref,
+    rows_ref,
+    cols_ref,
+    ng_ref,
+    routes_ref,
+    rweight_ref,
     hx_ref,
     kt_all,
     v_all,
@@ -128,6 +136,7 @@
     head_send,
     head_recv,
     load_sem,
+    early_sem,
     ring_send,
     ring_recv,
     plane_send,
@@ -188,6 +197,25 @@
         return (at(yy, j, core), tx)
 
     barrier = pltpu.get_barrier_semaphore()
+    early = [
+        pltpu.make_async_copy(src, dst, early_sem.at[i])
+        for i, (src, dst) in enumerate(
+            (
+                (k_hbm, k_ref),
+                (kg_hbm, kg_ref),
+                (rows_hbm.at[:, pl.ds(sp * 8, 8), :], rows_ref),
+                (cols_hbm, cols_ref),
+                (v_hbm, v_all.at[sp]),
+                (q_hbm, q_ref),
+                (qg_hbm, qg_ref),
+                (routes_hbm, routes_ref),
+                (rweight_hbm, rweight_ref),
+                (ng_hbm, ng_ref),
+            )
+        )
+    ]
+    for load in early:
+        load.start()
     peers = [(sib, tx)] + [ring_device(d, (mine[d] + i) % 4) for d in range(3) for i in (1, 2, 3)]
     for peer in peers:
         pl.semaphore_signal(barrier, inc=1, device_id=peer, device_id_type=MESH)
@@ -223,14 +251,15 @@
     def origin(dy, dz, c):
         return at(yy - dy + 4, zz - dz + 4, c)
 
+    for load in early:
+        load.wait()
     for r in range(8):
         sl = pl.ds(r * GRID_W, GRID_W)
         for i in range(2):
-            trig[i, sl, :] = rows_ref[i, pl.ds(sp * 8 + r, 1), :] + cols_ref[i]
+            trig[i, sl, :] = rows_ref[i, r : r + 1, :] + cols_ref[i]
 
     kr = normed_rotary(k_ref[...], kg_ref[...], trig[0], trig[1])
     kt_all[sp] = kr.T.astype(BF16)
-    v_all[sp] = v_ref[...]
     factor = math.log2(math.e) / math.sqrt(HD)
     for h in range(4):
         qr = normed_rotary(q_ref[:, h * HD : (h + 1) * HD], qg_ref[...], trig[0], trig[1])
@@ -496,37 +525,34 @@
     loads[0].wait()
     for load in loads[7:]:
         load.wait()
-    for h in range(4):
-        for step in (1, 2, 3):
-            head_copy(step, h, (tx + step) % 4).wait_recv()
-    for h in range(4):
-        for step in (1, 2, 3):
-            head_copy(step, h, tx).wait_send()
-    for kind, index in sent:
-        buf, recv = (kt_all, krecv) if kind == 0 else (v_all, vrecv)
-        pltpu.make_async_remote_copy(
-            src_ref=buf.at[sp],
-            dst_ref=buf.at[sp],
-            send_sem=send_sem.at[index],
-            recv_sem=recv.at[sp],
-            device_id=(sib, tx),
-            device_id_type=MESH,
-        ).wait_send()
-
-    heads = jnp.concatenate([hx_ref[j, h] for j in range(4) for h in range(4)], axis=1)
+    def project(d, pair):
+        lo, hi = COLS[d]
+        parts = []
+        for j in range(4):
+            buf = (back[d], sending[d])[j // 2]
+            first = (j % 2) * 16 + pair * 8
+            parts.append(buf[first : first + 8].reshape(256, hi - lo))
+        weight = jnp.concatenate(parts, axis=0)
+        some = [hx_ref[j, 2 * pair + h] for j in range(4) for h in range(2)]
+        return jnp.dot(jnp.concatenate(some, axis=1), weight, preferred_element_type=F32)
+
     square = jnp.zeros((128, 128), F32)
-    for d in range(3):
-        lo, hi = COLS[d]
-        weight = jnp.concatenate(
-            [back[d][...].reshape(1024, hi - lo), sending[d][...].reshape(1024, hi - lo)], axis=0
-        )
-        part = jnp.dot(heads, weight, preferred_element_type=F32)
-        h1 = (residual[:, lo:hi].astype(F32) + part).astype(BF16)
-        hidden[:, lo:hi] = h1
-        hf = h1.astype(F32)
-        hf = hf * hf
-        for j in range((hi - lo) // 128):
-            square = square + hf[:, j * 128 : (j + 1) * 128]
+    for pair in range(2):
+        for h in (2 * pair, 2 * pair + 1):
+            for step in (1, 2, 3):
+                head_copy(step, h, (tx + step) % 4).wait_recv()
+        for d in range(3):
+            lo, hi = COLS[d]
+            if pair == 0:
+                shared[:, lo:hi] = project(d, 0)
+                continue
+            part = shared[:, lo:hi] + project(d, 1)
+            h1 = (residual[:, lo:hi].astype(F32) + part).astype(BF16)
+            hidden[:, lo:hi] = h1
+            hf = h1.astype(F32)
+            hf = hf * hf
+            for j in range((hi - lo) // 128):
+                square = square + hf[:, j * 128 : (j + 1) * 128]
     scale = lax.rsqrt(jnp.sum(square, axis=1, keepdims=True) * (1.0 / 2048.0) + EPS)
     for d in range(3):
         lo, hi = COLS[d]
@@ -544,8 +570,10 @@
             device_id_type=MESH,
         )
 
-    def spray(order, phase):
-        for i, (da, db, dc) in enumerate(order):
+    def spray(group, phase):
+        for i, (da, db, dc) in enumerate(GROUPED):
+            if da != group:
+                continue
             c = (core + dc) % 2
             plane_copy(0, ((zz + da) % 4) * 8 + ((yy + db) % 4) * 2 + c, i, phase).start()
             plane_copy(1, ((zz + da) % 4) * 8 + c * 4 + (tx + db) % 4, i, phase).start()
@@ -562,17 +590,14 @@
 
     def plane_arrived(d, q, phase):
         buf = (got, back)[phase][d]
-
-        @pl.when(q != place_of[d])
-        def _():
-            pltpu.make_async_remote_copy(
-                src_ref=buf.at[q],
-                dst_ref=buf.at[q],
-                send_sem=plane_send.at[phase, d, 0],
-                recv_sem=plane_recv.at[phase, d, q],
-                device_id=plane_device(d, (place_of[d] + 1) % 32),
-                device_id_type=MESH,
-            ).wait_recv()
+        pltpu.make_async_remote_copy(
+            src_ref=buf.at[q],
+            dst_ref=buf.at[q],
+            send_sem=plane_send.at[phase, d, 0],
+            recv_sem=plane_recv.at[phase, d, q],
+            device_id=plane_device(d, (place_of[d] + 1) % 32),
+            device_id_type=MESH,
+        ).wait_recv()
 
     def each(lo, hi, act):
         def go(i, carry):
@@ -582,15 +607,22 @@
         lax.fori_loop(lo, hi, go, 0)
 
     for d in range(3):
-        width = COLS[d][1] - COLS[d][0]
         for i in (1, 2, 3):
             ring_arrived(near[d], d, i, 1)
-        for pair in range(2):
-            rows = near[d][2 * pair : 2 * pair + 2].reshape(256, width)
-            moved = jnp.dot(place[d, pair], rows, preferred_element_type=F32).astype(BF16)
-            sending[d][:, pair * 16 : (pair + 1) * 16, :] = moved.reshape(32, 16, width)
+    for step in (2, 1, 3, 0):
+        for d in range(3):
+            width = COLS[d][1] - COLS[d][0]
+            g = ((zz, zz, yy)[d] + step) % 4
+            for pair in range(2):
+                rows = near[d][2 * pair : 2 * pair + 2].reshape(256, width)
+                pick = place[d, pair, pl.ds(pl.multiple_of(g * 128, 128), 128), :]
+                moved = jnp.dot(pick, rows, preferred_element_type=F32).astype(BF16)
+                sending[d][pl.ds(g * 8, 8), pair * 16 : (pair + 1) * 16, :] = moved.reshape(
+                    8, 16, width
+                )
+        spray(step, 0)
+    for d in range(3):
         got[d][place_of[d]] = sending[d][place_of[d]]
-    spray(GROUPED, 0)
 
     for load in loads[1:7]:
         load.wait()
@@ -618,7 +650,15 @@
         for d in range(3):
             lo, hi = COLS[d]
             g = ((zz, zz, yy)[d] + step) % 4
-            each(0, 8, lambda q, d=d, g=g: plane_arrived(d, g * 8 + q, 0))
+            if step:
+                each(0, 8, lambda q, d=d, g=g: plane_arrived(d, g * 8 + q, 0))
+            else:
+                own = place_of[d] % 8
+                each(
+                    1,
+                    8,
+                    lambda q, d=d, g=g, own=own: plane_arrived(d, g * 8 + (own + q) % 8, 0),
+                )
             rows = got[d][pl.ds(g * 8, 8)].reshape(256, hi - lo)
             for n, weight in enumerate((gate, up)):
                 part = jnp.dot(rows, weight[lo:hi, :], preferred_element_type=F32)
@@ -639,16 +679,31 @@
         uu = (gsum[0, 1, sl] + gsum[1, 1, sl]).reshape(256, 256)
         hsum[sl] = (jax.nn.silu(gg) * uu).reshape(32, 8, 256)
     sprayed(0)
-    for d in range(3):
-        lo, hi = COLS[d]
-        for g in range(4):
+    for step in (2, 1, 3, 0):
+        for d in range(3):
+            lo, hi = COLS[d]
+            g = ((zz, zz, yy)[d] + step) % 4
             rows = jnp.concatenate(
                 [hsum[block_of(d, g, qi, j)] for qi in range(8) for j in range(4)], axis=0
             ).astype(BF16)
             result = jnp.dot(rows, down[:, lo:hi], preferred_element_type=F32).astype(BF16)
-            sending[d][g * 8 : g * 8 + 8] = result.reshape(8, 32, hi - lo)
+            sending[d][pl.ds(g * 8, 8)] = result.reshape(8, 32, hi - lo)
+        spray(step, 1)
+    for d in range(3):
         back[d][place_of[d]] = sending[d][place_of[d]]
-    spray(FARTHEST, 1)
+    for h in range(4):
+        for step in (1, 2, 3):
+            head_copy(step, h, tx).wait_send()
+    for kind, index in sent:
+        buf, recv = (kt_all, krecv) if kind == 0 else (v_all, vrecv)
+        pltpu.make_async_remote_copy(
+            src_ref=buf.at[sp],
+            dst_ref=buf.at[sp],
+            send_sem=send_sem.at[index],
+            recv_sem=recv.at[sp],
+            device_id=(sib, tx),
+            device_id_type=MESH,
+        ).wait_send()
 
     for d in range(3):
         for i in (1, 2, 3):
@@ -657,7 +712,7 @@
     for d in range(3):
         lo, hi = COLS[d]
         width = hi - lo
-        each(0, 32, lambda q, d=d: plane_arrived(d, q, 1))
+        each(1, 32, lambda q, d=d: plane_arrived(d, (place_of[d] + q) % 32, 1))
         for pair in range(2):
             rows = back[d][:, pair * 16 : (pair + 1) * 16, :].reshape(512, width)
             part = jnp.dot(mixw[d, pair], rows, preferred_element_type=F32).astype(BF16)
@@ -688,9 +743,18 @@
     return pl.pallas_call(
         layer_kernel,
         out_shape=jax.ShapeDtypeStruct((128, 2048), BF16),
-        in_specs=[vmem] * 10 + [hbm] * 8,
+        in_specs=[hbm] * 18,
         out_specs=vmem,
         scratch_shapes=[
+            pltpu.VMEM((TOK, 4 * HD), BF16),
+            pltpu.VMEM((TOK, HD), BF16),
+            pltpu.VMEM((1, HD), F32),
+            pltpu.VMEM((1, HD), F32),
+            pltpu.VMEM((2, 8, HD), F32),
+            pltpu.VMEM((2, GRID_W, HD), F32),
+            pltpu.VMEM((1, 2048), F32),
+            pltpu.VMEM((4, 128), jnp.int32),
+            pltpu.VMEM((4, 128), F32),
             pltpu.VMEM((4, 4, 128, HD), BF16),
             pltpu.VMEM((32, HD, TOK), BF16),
             pltpu.VMEM((32, TOK, HD), BF16),
@@ -725,6 +789,7 @@
             pltpu.SemaphoreType.DMA((4, 4)),
             pltpu.SemaphoreType.DMA((4, 4)),
             pltpu.SemaphoreType.DMA((13,)),
+            pltpu.SemaphoreType.DMA((10,)),
             pltpu.SemaphoreType.DMA((3, 3, 4)),
             pltpu.SemaphoreType.DMA((3, 3, 4)),
             pltpu.SemaphoreType.DMA((2, 3, 32)),

time: 169 us -> 172 us (1.018)
  Pallas kernels: 167 us -> 170 us
    pallas_call x1, Pallas kernels: 167 us -> 170 us  [layer(): pl.pallas_call(layer_kernel, out_shape=jax.ShapeDtypeStruct((128, 2048),...]
where the time goes in v4:
time: 172 us
  Pallas kernels  170 us (99%)
  local copies, waits for them, and re-layouts  1.88 us (1%)
    pallas_call x1, Pallas kernels, layer(): pl.pallas_call(layer_kernel, out_shape=jax.ShapeDtypeStruct((128, 2048),...  170 us

profile of v4, /device:TPU:1, one launch (start us, length us, event | category | flops | bytes accessed | tf_op | source)
XLA Modules:
  0.0 171.5 jit_solution(5061385557806797783)
XLA Ops:
  0.0 169.6 %layer.1 = bf16[128,2048]{1,0:T(8,128)(2,1)} custom-call(bf16[512,512]{1,0:T(8,128)(2,1)} %q_hbm.1, bf16[512,128]{1,0:T(8,128)(2,1)} %k_hbm.1, bf16[512,128]{1,0:T(8,128)(2,1)} %v_hbm.1, f32[1,128]{1,0:T(1,128)} %bitcast.10, f32[1,128]{1,0:T(1,128)} %bitcast.11, f32[2,256,128]{2,1,0:T(8,128)} %constant.4.clone.rows_hbm, ...), custom_call_target="tpu_custom_call" | custom-call | tf_op jit(solution)/shard_map/layer/pallas_call | solution.py:743
  169.7 1.9 %copy.20 = bf16[128,2048]{1,0:T(8,128)(2,1)} copy(bf16[128,2048]{1,0:T(8,128)(2,1)} %layer.1) | data formatting | bytes 1048576

commit v5 on v3

--- a/solution.py
+++ b/solution.py
@@ -496,9 +496,96 @@
     loads[0].wait()
     for load in loads[7:]:
         load.wait()
-    for h in range(4):
-        for step in (1, 2, 3):
-            head_copy(step, h, (tx + step) % 4).wait_recv()
+    def project(d, pair):
+        lo, hi = COLS[d]
+        parts = []
+        for j in range(4):
+            buf = (back[d], sending[d])[j // 2]
+            first = (j % 2) * 16 + pair * 8
+            parts.append(buf[first : first + 8].reshape(256, hi - lo))
+        weight = jnp.concatenate(parts, axis=0)
+        some = [hx_ref[j, 2 * pair + h] for j in range(4) for h in range(2)]
+        return jnp.dot(jnp.concatenate(some, axis=1), weight, preferred_element_type=F32)
+
+    square = jnp.zeros((128, 128), F32)
+    for pair in range(2):
+        for h in (2 * pair, 2 * pair + 1):
+            for step in (1, 2, 3):
+                head_copy(step, h, (tx + step) % 4).wait_recv()
+        for d in range(3):
+            lo, hi = COLS[d]
+            if pair == 0:
+                shared[:, lo:hi] = project(d, 0)
+                continue
+            part = shared[:, lo:hi] + project(d, 1)
+            h1 = (residual[:, lo:hi].astype(F32) + part).astype(BF16)
+            hidden[:, lo:hi] = h1
+            hf = h1.astype(F32)
+            hf = hf * hf
+            for j in range((hi - lo) // 128):
+                square = square + hf[:, j * 128 : (j + 1) * 128]
+    scale = lax.rsqrt(jnp.sum(square, axis=1, keepdims=True) * (1.0 / 2048.0) + EPS)
+    for d in range(3):
+        lo, hi = COLS[d]
+        near[d][mine[d]] = (hidden[:, lo:hi].astype(F32) * scale * ng_ref[:, lo:hi]).astype(BF16)
+        for i in (1, 2, 3):
+            ring_copy(near[d], None, d, i, 1).start()
+
+    def plane_copy(d, q, i, phase):
+        return pltpu.make_async_remote_copy(
+            src_ref=sending[d].at[q],
+            dst_ref=(got, back)[phase][d].at[place_of[d]],
+            send_sem=plane_send.at[phase, d, i],
+            recv_sem=plane_recv.at[phase, d, place_of[d]],
+            device_id=plane_device(d, q),
+            device_id_type=MESH,
+        )
+
+    def spray(order, phase):
+        for i, (da, db, dc) in enumerate(order):
+            c = (core + dc) % 2
+            plane_copy(0, ((zz + da) % 4) * 8 + ((yy + db) % 4) * 2 + c, i, phase).start()
+            plane_copy(1, ((zz + da) % 4) * 8 + c * 4 + (tx + db) % 4, i, phase).start()
+            plane_copy(2, ((yy + da) % 4) * 8 + c * 4 + (tx + db) % 4, i, phase).start()
+
+    def sprayed(phase):
+        for d in range(3):
+
+            def go(i, carry, d=d):
+                plane_copy(d, (place_of[d] + 1) % 32, i, phase).wait_send()
+                return carry
+
+            lax.fori_loop(0, 31, go, 0)
+
+    def plane_arrived(d, q, phase):
+        buf = (got, back)[phase][d]
+        pltpu.make_async_remote_copy(
+            src_ref=buf.at[q],
+            dst_ref=buf.at[q],
+            send_sem=plane_send.at[phase, d, 0],
+            recv_sem=plane_recv.at[phase, d, q],
+            device_id=plane_device(d, (place_of[d] + 1) % 32),
+            device_id_type=MESH,
+        ).wait_recv()
+
+    def each(lo, hi, act):
+        def go(i, carry):
+            act(i)
+            return carry
+
+        lax.fori_loop(lo, hi, go, 0)
+
+    for d in range(3):
+        width = COLS[d][1] - COLS[d][0]
+        for i in (1, 2, 3):
+            ring_arrived(near[d], d, i, 1)
+        for pair in range(2):
+            rows = near[d][2 * pair : 2 * pair + 2].reshape(256, width)
+            moved = jnp.dot(place[d, pair], rows, preferred_element_type=F32).astype(BF16)
+            sending[d][:, pair * 16 : (pair + 1) * 16, :] = moved.reshape(32, 16, width)
+        got[d][place_of[d]] = sending[d][place_of[d]]
+    spray(GROUPED, 0)
+
     for h in range(4):
         for step in (1, 2, 3):
             head_copy(step, h, tx).wait_send()
@@ -512,86 +599,6 @@
             device_id=(sib, tx),
             device_id_type=MESH,
         ).wait_send()
-
-    heads = jnp.concatenate([hx_ref[j, h] for j in range(4) for h in range(4)], axis=1)
-    square = jnp.zeros((128, 128), F32)
-    for d in range(3):
-        lo, hi = COLS[d]
-        weight = jnp.concatenate(
-            [back[d][...].reshape(1024, hi - lo), sending[d][...].reshape(1024, hi - lo)], axis=0
-        )
-        part = jnp.dot(heads, weight, preferred_element_type=F32)
-        h1 = (residual[:, lo:hi].astype(F32) + part).astype(BF16)
-        hidden[:, lo:hi] = h1
-        hf = h1.astype(F32)
-        hf = hf * hf
-        for j in range((hi - lo) // 128):
-            square = square + hf[:, j * 128 : (j + 1) * 128]
-    scale = lax.rsqrt(jnp.sum(square, axis=1, keepdims=True) * (1.0 / 2048.0) + EPS)
-    for d in range(3):
-        lo, hi = COLS[d]
-        near[d][mine[d]] = (hidden[:, lo:hi].astype(F32) * scale * ng_ref[:, lo:hi]).astype(BF16)
-        for i in (1, 2, 3):
-            ring_copy(near[d], None, d, i, 1).start()
-
-    def plane_copy(d, q, i, phase):
-        return pltpu.make_async_remote_copy(
-            src_ref=sending[d].at[q],
-            dst_ref=(got, back)[phase][d].at[place_of[d]],
-            send_sem=plane_send.at[phase, d, i],
-            recv_sem=plane_recv.at[phase, d, place_of[d]],
-            device_id=plane_device(d, q),
-            device_id_type=MESH,
-        )
-
-    def spray(order, phase):
-        for i, (da, db, dc) in enumerate(order):
-            c = (core + dc) % 2
-            plane_copy(0, ((zz + da) % 4) * 8 + ((yy + db) % 4) * 2 + c, i, phase).start()
-            plane_copy(1, ((zz + da) % 4) * 8 + c * 4 + (tx + db) % 4, i, phase).start()
-            plane_copy(2, ((yy + da) % 4) * 8 + c * 4 + (tx + db) % 4, i, phase).start()
-
-    def sprayed(phase):
-        for d in range(3):
-
-            def go(i, carry, d=d):
-                plane_copy(d, (place_of[d] + 1) % 32, i, phase).wait_send()
-                return carry
-
-            lax.fori_loop(0, 31, go, 0)
-
-    def plane_arrived(d, q, phase):
-        buf = (got, back)[phase][d]
-
-        @pl.when(q != place_of[d])
-        def _():
-            pltpu.make_async_remote_copy(
-                src_ref=buf.at[q],
-                dst_ref=buf.at[q],
-                send_sem=plane_send.at[phase, d, 0],
-                recv_sem=plane_recv.at[phase, d, q],
-                device_id=plane_device(d, (place_of[d] + 1) % 32),
-                device_id_type=MESH,
-            ).wait_recv()
-
-    def each(lo, hi, act):
-        def go(i, carry):
-            act(i)
-            return carry
-
-        lax.fori_loop(lo, hi, go, 0)
-
-    for d in range(3):
-        width = COLS[d][1] - COLS[d][0]
-        for i in (1, 2, 3):
-            ring_arrived(near[d], d, i, 1)
-        for pair in range(2):
-            rows = near[d][2 * pair : 2 * pair + 2].reshape(256, width)
-            moved = jnp.dot(place[d, pair], rows, preferred_element_type=F32).astype(BF16)
-            sending[d][:, pair * 16 : (pair + 1) * 16, :] = moved.reshape(32, 16, width)
-        got[d][place_of[d]] = sending[d][place_of[d]]
-    spray(GROUPED, 0)
-
     for load in loads[1:7]:
         load.wait()
     gpart = jnp.zeros((128, 256), F32)
@@ -618,7 +625,15 @@
         for d in range(3):
             lo, hi = COLS[d]
             g = ((zz, zz, yy)[d] + step) % 4
-            each(0, 8, lambda q, d=d, g=g: plane_arrived(d, g * 8 + q, 0))
+            if step:
+                each(0, 8, lambda q, d=d, g=g: plane_arrived(d, g * 8 + q, 0))
+            else:
+                own = place_of[d] % 8
+                each(
+                    1,
+                    8,
+                    lambda q, d=d, g=g, own=own: plane_arrived(d, g * 8 + (own + q) % 8, 0),
+                )
             rows = got[d][pl.ds(g * 8, 8)].reshape(256, hi - lo)
             for n, weight in enumerate((gate, up)):
                 part = jnp.dot(rows, weight[lo:hi, :], preferred_element_type=F32)
@@ -657,7 +672,7 @@
     for d in range(3):
         lo, hi = COLS[d]
         width = hi - lo
-        each(0, 32, lambda q, d=d: plane_arrived(d, q, 1))
+        each(1, 32, lambda q, d=d: plane_arrived(d, (place_of[d] + q) % 32, 1))
         for pair in range(2):
             rows = back[d][:, pair * 16 : (pair + 1) * 16, :].reshape(512, width)
             part = jnp.dot(mixw[d, pair], rows, preferred_element_type=F32).astype(BF16)

time: 169 us -> 168 us (level)
  no operation moved by 1% of the time
where the time goes in v5:
time: 168 us
  Pallas kernels  166 us (99%)
  local copies, waits for them, and re-layouts  1.88 us (1%)
    pallas_call x1, Pallas kernels, layer(): pl.pallas_call(layer_kernel, out_shape=jax.ShapeDtypeStruct((128, 2048),...  166 us

profile of v5, /device:TPU:1, one launch (start us, length us, event | category | flops | bytes accessed | tf_op | source)
XLA Modules:
  0.0 167.8 jit_solution(10197870762035592265)
XLA Ops:
  0.0 165.9 %layer.1 = bf16[128,2048]{1,0:T(8,128)(2,1)} custom-call(bf16[512,512]{1,0:T(8,128)(2,1)} %q_ref.1, bf16[512,128]{1,0:T(8,128)(2,1)} %k_ref.1, bf16[512,128]{1,0:T(8,128)(2,1)} %v_ref.1, f32[1,128]{1,0:T(1,128)} %bitcast.10, f32[1,128]{1,0:T(1,128)} %bitcast.11, f32[2,256,128]{2,1,0:T(8,128)} %constant.4.clone.rows_ref, ...), custom_call_target="tpu_custom_call" | custom-call | tf_op jit(solution)/shard_map/layer/pallas_call | solution.py:703
  165.9 1.9 %copy.20 = bf16[128,2048]{1,0:T(8,128)(2,1)} copy(bf16[128,2048]{1,0:T(8,128)(2,1)} %layer.1) | data formatting | bytes 1048576
